TPU v7x, 32 devices: a whole 2x2x4 slice. The times are simulated.
32 devices in a mesh: sp: 8 (over z, y), tp: 4 (over x, core).
Axes of the slice: x: 2, y: 2, z: 4, core: 2. Of those that a mesh axis runs over, the one named last changes fastest.
Arguments:
- input_activations: bfloat16 [8192, 2048], P(('sp', 'tp')), may hold values from -6 to 6
- norm_gain: float32 [2048], replicated, may hold values from 0.5 to 1.5
- w_gate: bfloat16 [2048, 2048], P('sp', 'tp'), may hold values from -0.125 to 0.125
- w_value: bfloat16 [2048, 2048], P('sp', 'tp'), may hold values from -0.125 to 0.125
- w_state_in: bfloat16 [2048, 1024], P('sp', 'tp'), may hold values from -0.125 to 0.125
- w_state_out: bfloat16 [2048, 1024], P('sp', 'tp'), may hold values from -0.125 to 0.125
- w_step_forward: bfloat16 [2048, 32], P('sp', 'tp'), may hold values from -0.03125 to 0.03125
- w_step_backward: bfloat16 [2048, 32], P('sp', 'tp'), may hold values from -0.03125 to 0.03125
- step_offset: float32 [2, 32], P(None, 'tp'), may hold values from -0.5 to 0.5
- fading_speed: float32 [2, 32], P(None, 'tp'), may hold values from 0.3 to 1
- conv_value: float32 [3, 2048], P(None, 'tp'), may hold values from -3.5 to 3.5
- conv_state_in: float32 [3, 1024], P(None, 'tp'), may hold values from -3.5 to 3.5
- conv_state_out: float32 [3, 1024], P(None, 'tp'), may hold values from -3.5 to 3.5
- out_gain: float32 [2048], P('tp'), may hold values from 0.5 to 1.5
- w_out: bfloat16 [2048, 2048], P('tp', 'sp'), may hold values from -0.125 to 0.125
Outputs:
- mixer_out: bfloat16 [8192, 2048], P(('sp', 'tp'))
All inputs are finite; a program needn't handle non-finite values.
Results may differ from a plain program's by a relative error of at most 0.015.
Values may be sent and summed in bfloat16 or wider, within the bound.
A program may use at most 128 MiB of HBM per device.

v0:
```python
import math

import jax
import jax.numpy as jnp
from jax import lax
from jax.sharding import PartitionSpec as P

HEAD_DIM = 64
STATE = 128
BLOCK = 128


epsilon = 1e-06
HIGHEST_PRECISION = lax.Precision.HIGHEST


def taken_in(section, axis, dim):

    def gathered(part):
        return lax.all_gather(part, axis, axis=dim, tiled=True)

    return jax.tree.map(gathered, section)


def for_sending(shard):
    def short(part):
        return part.astype(jnp.bfloat16) if part.dtype == jnp.float32 else part

    return jax.tree.map(short, shard)


def extended(block, sides, width, periodic):
    for axis, dim in sides:
        count = lax.axis_size(axis)
        forward = [(i, i + 1) for i in range(count - 1)]
        if periodic:
            forward.append((count - 1, 0))
        backward = [(target, source) for source, target in forward]
        low = lax.ppermute(
            lax.slice_in_dim(block, block.shape[dim] - width, None, axis=dim), axis, forward
        )
        high = lax.ppermute(lax.slice_in_dim(block, 0, width, axis=dim), axis, backward)
        block = jnp.concatenate([low, block, high], axis=dim)
    return block


def prefix(part, axis, combine, identity, reverse):
    count = lax.axis_size(axis)
    place = lax.axis_index(axis)
    ahead = count - 1 - place if reverse else place
    gathered = jax.tree.map(lambda a: lax.all_gather(a, axis), part)
    state = jax.tree.map(lambda a, e: jnp.zeros_like(a) + jnp.asarray(e, a.dtype), part, identity)

    def one(hop, state):
        source = count - 1 - hop if reverse else hop
        return combine(
            state, jax.tree.map(lambda a: lax.dynamic_index_in_dim(a, source, 0, False), gathered)
        )

    return lax.fori_loop(0, ahead, one, state)


def rms_rows(values):
    wide = values.astype(jnp.float32)
    return wide * lax.rsqrt(jnp.mean(wide * wide, axis=-1, keepdims=True) + epsilon)


def short_filter(padded, taps):
    wide = padded.astype(jnp.float32)
    mixed = taps[0] * wide[:-2] + taps[1] * wide[1:-1] + taps[2] * wide[2:]
    return jax.nn.silu(mixed).astype(jnp.bfloat16)


def one_way(signal, step_size, rate, inward, outward, intersect):
    sequence_extent, groups, ratio, width = signal.shape
    states = inward.shape[2]
    count = sequence_extent // BLOCK
    blocks = signal.reshape(count, BLOCK, groups, ratio, width).astype(jnp.float32)
    step_blocks = step_size.reshape(count, BLOCK, groups, ratio)
    within = jnp.cumsum(-step_blocks * rate, axis=1)
    final = within[:, -1]
    scaling_factor = jnp.exp(final[:, None] - within) * step_blocks
    inward_blocks = inward.reshape(count, BLOCK, groups, states).astype(jnp.float32)
    outward_blocks = outward.reshape(count, BLOCK, groups, states).astype(jnp.float32)
    block_states = jnp.einsum(
        "cqgn,cqgrp->cgrpn",
        inward_blocks,
        blocks * scaling_factor[..., None],
        precision=HIGHEST_PRECISION,
    )

    def advance(state, inputs):
        return (state * inputs[1][..., None, None] + inputs[0], state)

    start_state = jnp.zeros((groups, ratio, width, states), jnp.float32)
    last_state, before = lax.scan(advance, start_state, (block_states, jnp.exp(final)))
    lower = (jnp.arange(BLOCK)[:, None] >= jnp.arange(BLOCK)[None, :])[None, :, :, None, None]
    gaps = within[:, :, None] - within[:, None]
    decay = jnp.where(lower, jnp.exp(jnp.where(lower, gaps, 0.0)), 0.0)
    weights_mix = intersect[..., None] * decay * step_blocks[:, None]
    diagonal = jnp.einsum("cqkgr,ckgrp->cqgrp", weights_mix, blocks, precision=HIGHEST_PRECISION)
    carried = (
        jnp.einsum("cqgn,cgrpn->cqgrp", outward_blocks, before, precision=HIGHEST_PRECISION)
        * jnp.exp(within)[..., None]
    )
    running = jnp.cumsum(final, axis=0)
    from_start = (within + (running - final)[:, None]).reshape(sequence_extent, groups, ratio)
    outputs = (diagonal + carried).reshape(sequence_extent, groups, ratio, width)
    return (
        outputs,
        from_start,
        jnp.exp(running[-1]),
        last_state,
        outward_blocks.reshape(sequence_extent, groups, states),
    )


def read_in(outward_wide, incoming, from_start):
    return (
        jnp.einsum("lgn,grpn->lgrp", outward_wide, incoming, precision=HIGHEST_PRECISION)
        * jnp.exp(from_start)[..., None]
    )


def link(earlier, later):
    return (earlier[0] * later[0], earlier[1] * later[0][..., None, None] + later[1])


def combine_ways(ahead, behind, ahead_state, behind_state):
    forward = ahead[0] + read_in(ahead[4], ahead_state, ahead[1])
    backward = behind[0] + read_in(behind[4], behind_state, behind[1])
    return forward + backward[::-1]


def on_device(
    input_activations,
    norm_gain,
    w_gate,
    w_value,
    w_state_in,
    w_state_out,
    w_step_forward,
    w_step_backward,
    step_offset,
    fading_speed,
    conv_value,
    conv_state_in,
    conv_state_out,
    out_gain,
    w_out,
):
    normed = (rms_rows(input_activations) * norm_gain).astype(jnp.bfloat16)
    gathered = lax.all_gather(normed, "tp", axis=0, tiled=True)
    sequence_extent = gathered.shape[0]
    scaling_factors = (w_gate, w_value, w_state_in, w_state_out, w_step_forward, w_step_backward)
    blank_entries = tuple(
        (
            jnp.zeros((sequence_extent, scaling_factor.shape[1]), jnp.float32)
            for scaling_factor in scaling_factors
        )
    )

    def accumulate(totals, pieces):
        columns = lax.slice_in_dim(gathered, 0, pieces[0].shape[0], axis=1)
        return tuple(
            (
                total + jnp.dot(columns, piece, preferred_element_type=jnp.float32)
                for total, piece in zip(totals, pieces)
            )
        )

    mapped_output = accumulate(
        blank_entries,
        taken_in(
            (
                scaling_factors[0],
                scaling_factors[1],
                scaling_factors[2],
                scaling_factors[3],
                scaling_factors[4],
                scaling_factors[5],
            ),
            "sp",
            0,
        ),
    )
    gate, value, state_in, state_out, raw_forward, raw_backward = [
        part.astype(jnp.bfloat16) for part in mapped_output
    ]
    joined = jnp.concatenate([value, state_in, state_out], axis=1)
    padded = extended(for_sending(joined), (("sp", 0),), 1, False).astype(joined.dtype)
    taps = jnp.concatenate([conv_value, conv_state_in, conv_state_out], axis=1)
    filtered = short_filter(padded, taps)
    content_breadth = value.shape[1]
    state_width = state_in.shape[1]
    heads_local = raw_forward.shape[1]
    groups_local = state_width // STATE
    ratio = heads_local // groups_local
    signal = filtered[:, :content_breadth].reshape(sequence_extent, groups_local, ratio, HEAD_DIM)
    inward = filtered[:, content_breadth : content_breadth + state_width].reshape(
        sequence_extent, groups_local, STATE
    )
    outward = filtered[:, content_breadth + state_width :].reshape(
        sequence_extent, groups_local, STATE
    )
    shift = math.log(sequence_extent * lax.axis_size("sp"))
    forward_step = jax.nn.softplus(
        raw_forward.astype(jnp.float32) + step_offset[0] - shift
    ).reshape(sequence_extent, groups_local, ratio)
    backward_step = jax.nn.softplus(
        raw_backward.astype(jnp.float32) + step_offset[1] - shift
    ).reshape(sequence_extent, groups_local, ratio)
    rates = fading_speed.reshape(2, groups_local, ratio)
    count = sequence_extent // BLOCK
    intersect = jnp.einsum(
        "cqgn,ckgn->cqkg",
        outward.reshape(count, BLOCK, groups_local, STATE),
        inward.reshape(count, BLOCK, groups_local, STATE),
        preferred_element_type=jnp.float32,
    )
    flipped = intersect[::-1, ::-1, ::-1]
    ahead = one_way(signal, forward_step, rates[0], inward, outward, intersect)
    behind = one_way(
        signal[::-1], backward_step[::-1], rates[1], inward[::-1], outward[::-1], flipped
    )
    ahead_in = prefix(
        (ahead[2], ahead[3]), "sp", link, (jnp.ones_like(ahead[2]), jnp.zeros_like(ahead[3])), False
    )
    behind_in = prefix(
        (behind[2], behind[3]),
        "sp",
        link,
        (jnp.ones_like(behind[2]), jnp.zeros_like(behind[3])),
        True,
    )
    combined = combine_ways(ahead, behind, ahead_in[1], behind_in[1])
    gated = combined.reshape(sequence_extent, content_breadth) * jax.nn.silu(
        gate.astype(jnp.float32)
    )
    grouped = rms_rows(
        gated.reshape(sequence_extent, groups_local, content_breadth // groups_local)
    ).reshape(sequence_extent, content_breadth)
    mixed = (grouped * out_gain).astype(jnp.bfloat16)
    full_out = lax.all_gather(w_out, "sp", axis=1, tiled=True)

    def product(count):
        return jnp.dot(
            lax.slice_in_dim(mixed, 0, count, axis=0), full_out, preferred_element_type=jnp.float32
        )

    result = lax.psum_scatter(
        product(input_activations.shape[0] * lax.axis_size("tp")),
        "tp",
        scatter_dimension=0,
        tiled=True,
    )
    return result.astype(jnp.bfloat16)


def solution(mesh):
    return jax.shard_map(
        on_device,
        mesh=mesh,
        in_specs=(
            P(("sp", "tp"), None),
            P(),
            P("sp", "tp"),
            P("sp", "tp"),
            P("sp", "tp"),
            P("sp", "tp"),
            P("sp", "tp"),
            P("sp", "tp"),
            P(None, "tp"),
            P(None, "tp"),
            P(None, "tp"),
            P(None, "tp"),
            P(None, "tp"),
            P("tp"),
            P("tp", "sp"),
        ),
        out_specs=P(("sp", "tp"), None),
        check_vma=False,
    )
```

profile of v0, /device:TPU:0, one launch (start us, length us, event | category | flops | bytes accessed | tf_op | source)
XLA Modules:
  0.0 533.4 jit_solution(11527782727118973745)
XLA Ops:
  13.5 32.3 %all_gather.48 = bf16[2048,8]{0,1:T(8,128)(2,1)S(1)} all-gather(bf16[256,8]{0,1:T(8,128)(2,1)S(1)} %copy-done.30), channel_id=1, replica_groups=mesh['sp'=8,'tp'=4] {'sp'}, dimensions={0}, use_global_device_ids=true | all-gather | bytes 36864 | tf_op jit(solution)/shard_map/all_gather | solution.py:20
  45.9 30.4 %all_gather.52 = bf16[2048,8]{0,1:T(8,128)(2,1)S(1)} all-gather(bf16[256,8]{0,1:T(8,128)(2,1)S(1)} %copy-done.31), channel_id=1, replica_groups=mesh['sp'=8,'tp'=4] {'sp'}, dimensions={0}, use_global_device_ids=true | all-gather | bytes 36864 | tf_op jit(solution)/shard_map/all_gather | solution.py:20
  76.4 3.4 compare_select_fusion.1
  80.3 3.8 compare_select_fusion
  86.9 47.4 %fusion.77 = f32[8,128,2,4]{3,0,1,2:T(8,128)S(1)} fusion(f32[8,128,2,4]{3,0,1,2:T(8,128)S(1)} %copy.174), kind=kOutput, calls=%fused_computation.139 | output fusion | flops 1040384 | bytes 65536 | tf_op jit(solution)/shard_map/jit(cumsum)/reduce_window_sum | solution.py:80
  137.0 3.8 convolution_convert_fusion.2
  140.8 6.3 %convolution_convert_fusion.1 = bf16[1024,512]{0,1:T(8,128)(2,1)} fusion(bf16[1024,2048]{1,0:T(8,128)(2,1)} %all-gather.11.cloned.1.call-done, bf16[2048,512]{1,0:T(8,128)(2,1)} %all-gather.13.cloned.1.call-done), kind=kOutput, calls=%fused_computation.76 | convolution fusion | flops 2148007936 | bytes 7340032 | tf_op jit(solution)/shard_map/dot_general | solution.py:167
  147.1 35.1 %all-gather.15.cloned.1.call-done = bf16[2048,256]{1,0:T(8,128)(2,1)} async-done(((bf16[256,256]{1,0:T(8,128)(2,1)}), bf16[2048,256]{1,0:T(8,128)(2,1)}) %all-gather.15.cloned.1.call-update) | async-done | bytes 1048592 | tf_op jit(solution)/shard_map/all_gather | solution.py:20
  182.2 3.9 convolution_convert_fusion.3
  200.3 4.0 concatenate.11
  206.3 2.9 multiply_convert_fusion
  217.1 8.3 %rev.21 = bf16[1024,2,128]{2,0,1:T(8,128)(2,1)} reverse(bf16[1024,2,128]{2,0,1:T(8,128)(2,1)} %copy.183), dimensions={0} | reverse | bytes 1048576 | tf_op jit(solution)/shard_map/rev | solution.py:224
  226.4 2.6 fusion.30
  229.3 13.9 %while.55 = (s32[]{:T(128)}, f32[2,4,64,128]{3,2,1,0:T(8,128)S(1)}, f32[8,2,4,64,128]{4,3,2,1,0:T(8,128)S(1)}, f32[8,2,4]{2,1,0:T(2,128)}, f32[8,2,4,64,128]{4,3,2,1,0:T(8,128)}, /*index=5*/s32[]{:T(128)}, s32[]{:T(128)}) while((s32[]{:T(128)}, f32[2,4,64,128]{3,2,1,0:T(8,128)S(1)}, f32[8,2,4,64,128]{4,3,2,1,0:T(8,128)S(1)}, ...), condition=%wide.region_9.10_spmd.clone, body=%wide.region_8.9_spmd.clone.sunk | while | flops 262147 | bytes 1310916 | solution.py:96
  244.0 4.0 fusion.36
  249.6 19.5 %while.54 = (s32[]{:T(128)}, f32[2,4,64,128]{3,2,1,0:T(8,128)S(1)}, f32[8,2,4,64,128]{4,3,2,1,0:T(8,128)}, f32[8,2,4]{2,1,0:T(2,128)}, f32[8,2,4,64,128]{4,3,2,1,0:T(8,128)}, /*index=5*/s32[]{:T(128)}, s32[]{:T(128)}) while((s32[]{:T(128)}, f32[2,4,64,128]{3,2,1,0:T(8,128)S(1)}, f32[8,2,4,64,128]{4,3,2,1,0:T(8,128)}, ...), condition=%wide.region_3.4_spmd.clone, body=%wide.region_2.3_spmd.clone.sunk | while | flops 262147 | bytes 1311424 | solution.py:96
  275.5 20.5 %all_gather.53 = f32[8,2,4]{2,1,0:T(2,128)S(1)} all-gather(f32[1,2,4]{2,1,0:T(2,128)S(1)} %slice_exponential_fusion), channel_id=1, replica_groups=mesh['sp'=8,'tp'=4] {'sp'}, dimensions={0}, use_global_device_ids=true | all-gather | bytes 288 | tf_op jit(solution)/shard_map/all_gather | solution.py:51
  296.4 16.6 %all_gather.49 = f32[8,2,4]{2,1,0:T(2,128)S(1)} all-gather(f32[1,2,4]{2,1,0:T(2,128)S(1)} %slice_exponential_fusion.1), channel_id=1, replica_groups=mesh['sp'=8,'tp'=4] {'sp'}, dimensions={0}, use_global_device_ids=true | all-gather | bytes 288 | tf_op jit(solution)/shard_map/all_gather | solution.py:51
  316.2 5.8 %rev.19 = f32[8,128,128,2]{1,2,3,0:T(8,128)} reverse(f32[8,128,128,2]{1,2,3,0:T(8,128)S(1)} %convolution_bitcast_fusion), dimensions={0,1,2} | reverse | bytes 2097152 | tf_op jit(solution)/shard_map/rev | solution.py:221
  322.0 2.6 copy.173
  325.6 6.1 %fusion.9 = f32[8,2,4,64,128]{4,3,2,1,0:T(8,128)S(1)} fusion(f32[8,128,2,4]{1,3,2,0:T(4,128)S(1)} %bitcast.221, f32[8,128,2,4]{1,3,2,0:T(4,128)S(1)} %copy.152, f32[8,128,128,2]{2,1,3,0:T(8,128)} %copy.150, pred[128,128]{1,0:T(8,128)(4,1)S(1)} %iota_compare_fusion, bf16[8,128,2,4,64]{1,0,4,3,2:T(8,128)(2,1)S(1)} %bitcast.212), kind=kOutput, calls=%fused_computation.22 | convolution fusion | flops 810549248 | bytes 4276224 | tf_op jit(solution)/shard_map/cqkgr,ckgrp->cqgrp/dot_general | solution.py:101
  331.7 4.6 fusion.2
  340.5 8.0 %while.53 = (s32[]{:T(128)}, f32[2,4,64,128]{3,2,1,0:T(8,128)S(1)}, s32[]{:T(128)}, f32[8,2,4]{2,1,0:T(2,128)S(1)}, f32[8,2,4,64,128]{4,3,2,1,0:T(8,128)}, /*index=5*/s32[]{:T(128)}, s32[]{:T(128)}, s32[]{:T(128)}, s32[]{:T(128)}) while((s32[]{:T(128)}, f32[2,4,64,128]{3,2,1,0:T(8,128)S(1)}, s32[]{:T(128)}, f32[8,2,4]{2,1,0:T(2,128)S(1)}, ...), condition=%wide.region_12.13_spmd, body=%wide.region_11.12_spmd.sunk | while | flops 131078 | bytes 786675 | solution.py:60
  348.5 4.1 bitcast_add_fusion.4
  352.7 6.1 %rev.23 = f32[1024,2,4,64]{0,3,2,1:T(8,128)} reverse(f32[1024,2,4,64]{0,3,2,1:T(8,128)} %bitcast_add_fusion.4), dimensions={0} | reverse | bytes 4194304 | tf_op jit(solution)/shard_map/rev | solution.py:132
  358.8 4.0 fusion.23
  362.9 32.7 %all-gather.19.cloned.1.call-done = bf16[2048,512]{1,0:T(8,128)(2,1)} async-done(((bf16[256,512]{1,0:T(8,128)(2,1)}), bf16[2048,512]{1,0:T(8,128)(2,1)}) %all-gather.19.cloned.1.call-update) | async-done | bytes 2097168 | tf_op jit(solution)/shard_map/all_gather | solution.py:20
  395.6 6.3 %bitcast_reduce_fusion = (f32[1024,2]{0,1:T(2,128)S(1)}, f32[1024,512]{0,1:T(8,128)S(1)}) fusion(bf16[1024,2048]{1,0:T(8,128)(2,1)} %all-gather.11.cloned.1.call-done, bf16[2048,512]{1,0:T(8,128)(2,1)} %all-gather.19.cloned.1.call-done, f32[1024,2,4,64]{0,3,2,1:T(8,128)} %fusion.23), kind=kOutput, calls=%fused_computation.48 | convolution fusion | flops 2152200192 | bytes 10493952 | tf_op jit(solution)/shard_map/dot_general | solution.py:167
  402.1 44.6 %all-gather.21.cloned.1.call-done = bf16[512,2048]{1,0:T(8,128)(2,1)} async-done(((bf16[512,256]{1,0:T(8,128)(2,1)}), bf16[512,2048]{1,0:T(8,128)(2,1)}) %all-gather.21.cloned.1.call-update) | async-done | bytes 2097168 | tf_op jit(solution)/shard_map/all_gather | solution.py:244
  446.7 7.3 %fusion.79 = f32[1024,2048]{1,0:T(8,128)} fusion(bf16[1024,512]{0,1:T(8,128)(2,1)S(1)} %fusion.25, bf16[512,2048]{1,0:T(8,128)(2,1)} %all-gather.21.cloned.1.call-done), kind=kOutput, calls=%fused_computation.141 | convolution fusion | flops 2147483648 | bytes 11534336 | tf_op jit(solution)/shard_map/dot_general | solution.py:247
  454.0 69.7 %reduce-scatter.2.cloned.1.call-done = f32[256,2048]{1,0:T(8,128)} async-done(((f32[1024,2048]{1,0:T(8,128)}), f32[256,2048]{1,0:T(8,128)}) %reduce-scatter.2.cloned.1.call-update) | async-done | bytes 2097168 | tf_op jit(solution)/shard_map/reduce_scatter | solution.py:251
  523.7 2.7 convert_element_type.71
  (242 shorter events, 96.1 us)
Async XLA Ops:
  6.5 69.9 %all-gather.11.cloned.1.call-start = ((), (), s32[]{:S(2)}) async-start(), calls=%async_computation.1 | async-start | bytes 5242880 | tf_op jit(solution)/shard_map/all_gather | solution.py:153
  8.0 4.8 copy-start.29
  8.1 4.8 copy-start.32
  8.1 4.8 copy-start.33
  8.1 5.4 %copy-start.35 = (f32[2,8]{1,0:T(2,128)S(1)}, f32[2,8]{1,0:T(2,128)}, u32[]{:S(2)}) copy-start(f32[2,8]{1,0:T(2,128)} %param.31) | copy-start | bytes 196
  8.1 5.4 %copy-start.30 = (bf16[256,8]{0,1:T(8,128)(2,1)S(1)}, bf16[256,8]{0,1:T(8,128)(2,1)}, u32[]{:S(2)}) copy-start(bf16[256,8]{0,1:T(8,128)(2,1)} %param.29) | copy-start | bytes 12292
  8.1 37.7 %copy-start.36 = (f32[2,8]{1,0:T(2,128)S(1)}, f32[2,8]{1,0:T(2,128)}, u32[]{:S(2)}) copy-start(f32[2,8]{1,0:T(2,128)} %param.32) | copy-start | bytes 196
  8.1 37.8 %copy-start.31 = (bf16[256,8]{0,1:T(8,128)(2,1)S(1)}, bf16[256,8]{0,1:T(8,128)(2,1)}, u32[]{:S(2)}) copy-start(bf16[256,8]{0,1:T(8,128)(2,1)} %param.30) | copy-start | bytes 12292
  10.7 126.3 %all-gather.17.cloned.1.call-start = ((), (), s32[]{:S(2)}) async-start(), calls=%async_computation.4 | async-start | bytes 1179648 | tf_op jit(solution)/shard_map/all_gather | solution.py:20
  11.4 129.3 %all-gather.13.cloned.1.call-start = ((), (), s32[]{:S(2)}) async-start(), calls=%async_computation.2 | async-start | bytes 2359296 | tf_op jit(solution)/shard_map/all_gather | solution.py:20
  12.2 170.0 %all-gather.15.cloned.1.call-start = ((), (), s32[]{:S(2)}) async-start(), calls=%async_computation.3 | async-start | bytes 1179648 | tf_op jit(solution)/shard_map/all_gather | solution.py:20
  12.7 327.8 %all-gather.25.cloned.1.call-start = ((), (), s32[]{:S(2)}) async-start(), calls=%async_computation.9 | async-start | bytes 2359296 | tf_op jit(solution)/shard_map/all_gather | solution.py:51
  186.0 4.9 copy-start.3
  186.0 4.9 copy-start.6
  186.1 4.9 copy-start.9
  187.1 13.2 %collective-permute-start = (bf16[1,1024]{0,1:T(8,128)(2,1)}, bf16[1,1024]{0,1:T(8,128)(2,1)S(1)}, u32[]{:S(2)}, u32[]{:S(2)}) collective-permute-start(bf16[1,1024]{0,1:T(8,128)(2,1)} %get-tuple-element.340), channel_id=1, source_target_pairs={{0,4},{4,8},{8,12},{12,16},{16,20},{20,24},{24,28},{1,5},{5,9},{9,... | collective-permute-start | bytes 6152 | tf_op jit(solution)/shard_map/ppermute | solution.py:39
  189.4 10.9 %collective-permute-start.1 = (bf16[1,1024]{0,1:T(8,128)(2,1)S(1)}, bf16[1,1024]{0,1:T(8,128)(2,1)S(1)}, u32[]{:S(2)}, u32[]{:S(2)}) collective-permute-start(bf16[1,1024]{0,1:T(8,128)(2,1)S(1)} %get-tuple-element.339), channel_id=1, source_target_pairs={{4,0},{8,4},{12,8},{16,12},{20,16},{24,20},{28,24},{5,1},{9,5},{13... | collective-permute-start | bytes 6152 | tf_op jit(solution)/shard_map/ppermute | solution.py:42
  214.6 10.7 %copy-start.21 = (bf16[1024,2,4,64]{0,3,2,1:T(8,128)(2,1)}, bf16[1024,2,4,64]{0,3,2,1:T(8,128)(2,1)S(1)}, u32[]{:S(2)}) copy-start(bf16[1024,2,4,64]{0,3,2,1:T(8,128)(2,1)S(1)} %rev.18) | copy-start | bytes 3145732
  243.3 6.3 %copy-start.10 = (f32[8,2,4,64,128]{4,3,2,1,0:T(8,128)}, f32[8,2,4,64,128]{4,3,2,1,0:T(8,128)S(1)}, u32[]{:S(2)}) copy-start(f32[8,2,4,64,128]{4,3,2,1,0:T(8,128)S(1)} %get-tuple-element.192) | copy-start | bytes 6291460
  244.0 114.8 %all-gather.23.cloned.1.call-start = ((), (), s32[]{:S(2)}) async-start(), calls=%async_computation.8 | async-start | bytes 2359296 | tf_op jit(solution)/shard_map/all_gather | solution.py:51
  249.6 21.8 %copy-start.4 = (f32[8,128,2,4]{3,0,1,2:T(8,128)S(1)}, f32[8,128,2,4]{3,0,1,2:T(8,128)}, u32[]{:S(2)}) copy-start(f32[8,128,2,4]{3,0,1,2:T(8,128)} %copy-done.2) | copy-start | bytes 98308
  269.8 125.8 %all-gather.19.cloned.1.call-start = ((), (), s32[]{:S(2)}) async-start(), calls=%async_computation.5 | async-start | bytes 2359296 | tf_op jit(solution)/shard_map/all_gather | solution.py:20
  270.6 176.1 %all-gather.21.cloned.1.call-start = ((), (), s32[]{:S(2)}) async-start(), calls=%async_computation.6 | async-start | bytes 2359296 | tf_op jit(solution)/shard_map/all_gather | solution.py:244
  271.3 252.4 %reduce-scatter.2.cloned.1.call-start = ((), (), s32[]{:S(2)}) async-start(), calls=%async_computation.7 | async-start | bytes 10485760 | tf_op jit(solution)/shard_map/reduce_scatter | solution.py:251
  271.8 41.2 %copy-start.17 = (f32[8,128,2,4]{3,0,1,2:T(8,128)S(1)}, f32[8,128,2,4]{3,0,1,2:T(8,128)}, u32[]{:S(2)}) copy-start(f32[8,128,2,4]{3,0,1,2:T(8,128)} %get-tuple-element.341) | copy-start | bytes 98308
  272.2 23.8 %copy-start.18 = (f32[8,128,2,4]{3,0,1,2:T(8,128)S(1)}, f32[8,128,2,4]{3,0,1,2:T(8,128)}, u32[]{:S(2)}) copy-start(f32[8,128,2,4]{3,0,1,2:T(8,128)} %get-tuple-element.344) | copy-start | bytes 98308
  273.9 40.7 %copy-start.13 = (bf16[32,8,8,128]{3,2,1,0:T(8,128)(2,1)S(1)}, bf16[32,8,8,128]{3,2,1,0:T(8,128)(2,1)}, u32[]{:S(2)}) copy-start(bf16[32,8,8,128]{3,2,1,0:T(8,128)(2,1)} %copy.224) | copy-start | bytes 1572868
  325.5 12.1 %copy-start.14 = (bf16[1024,2,128]{2,0,1:T(8,128)(2,1)}, bf16[1024,2,128]{2,0,1:T(8,128)(2,1)S(1)}, u32[]{:S(2)}) copy-start(bf16[1024,2,128]{2,0,1:T(8,128)(2,1)S(1)} %rev.22) | copy-start | bytes 1572868
  325.6 6.1 %copy-start.22 = (bf16[1024,2,4,64]{0,3,2,1:T(8,128)(2,1)S(1)}, bf16[1024,2,4,64]{0,3,2,1:T(8,128)(2,1)}, u32[]{:S(2)}) copy-start(bf16[1024,2,4,64]{0,3,2,1:T(8,128)(2,1)} %copy-done.21) | copy-start | bytes 3145732
  325.6 6.1 %copy-start.24 = (f32[8,128,128,2]{2,1,3,0:T(8,128)S(1)}, f32[8,128,128,2]{2,1,3,0:T(8,128)}, u32[]{:S(2)}) copy-start(f32[8,128,128,2]{2,1,3,0:T(8,128)} %copy.173) | copy-start | bytes 3145732
  331.7 4.7 copy-start.12
  362.9 39.0 %copy-start.34 = (f32[512]{0:T(512)S(1)}, f32[512]{0:T(512)}, u32[]{:S(2)}) copy-start(f32[512]{0:T(512)} %param.36) | copy-start | bytes 6148
  (16 other events, 34.0 us)
Sparse Core Ops, SparseCore 0:
  10.8 37.0 all-gather.10
  50.1 40.6 all-gather.16
  92.9 47.7 all-gather.12
  142.7 39.4 all-gather.14
  244.1 51.0 all-gather.24
  297.1 48.1 all-gather.22
  347.5 48.0 all-gather.18
  397.6 49.0 all-gather.20
  454.1 69.5 reduce-scatter.1
where the time goes:
time: 543 us; the launch traced here: 533 us
  waiting for transfers between devices  186 us (34%)
  blocking collectives  99.8 us (18%)
  other arithmetic  93.7 us (17%)
  local copies, waits for them, and re-layouts  70.7 us (13%)
  matrix products  64.3 us (12%)
  between operations  14.4 us (3%)
    reduce_scatter x1, waiting for transfers between devices, on_device(): lax.psum_scatter(product(input_activations.shape[0] * lax.axis_size('tp')...  69.7 us
    all_gather x4, waiting for transfers between devices, gathered(): return lax.all_gather(part, axis, axis=dim, tiled=True)  67.9 us
    all_gather x2, blocking collectives, gathered(): return lax.all_gather(part, axis, axis=dim, tiled=True)  62.7 us
    another operation x2, other arithmetic, one_way(): within = jnp.cumsum(-step_blocks * rate, axis=1)  47.8 us
    all_gather x1, waiting for transfers between devices, on_device(): full_out = lax.all_gather(w_out, 'sp', axis=1, tiled=True)  44.6 us
    all_gather x2, blocking collectives, prefix(): gathered = jax.tree.map(lambda a: lax.all_gather(a, axis), part)  37.1 us
    dot_general x6, matrix products, accumulate(): jnp.dot(columns, piece, preferred_element_type=jnp.float32)  27.3 us
    add x16, other arithmetic, advance(): return (state * inputs[1][..., None, None] + inputs[0], state)  16.6 us
  transfers between devices with their start and end apart: 11, of which 4 were waited for; matrix products, arithmetic and copies ran while one was open for 31% of the time, Pallas kernels for 0%

commit v1 on v0

v1 whole, which is shorter than its diff:
```python
import functools
import math

import jax
import jax.numpy as jnp
from jax import lax
from jax.experimental import pallas as pl
from jax.experimental.pallas import tpu as pltpu
from jax.sharding import PartitionSpec as P

HEAD_DIM = 64
STATE = 128
BLOCK = 128
LANES = 128
EPSILON = 1e-06
HIGHEST = lax.Precision.HIGHEST
VMEM_LIMIT = 60 * 1024 * 1024


def rms_rows(values):
    wide = values.astype(jnp.float32)
    return wide * lax.rsqrt(jnp.mean(wide * wide, axis=-1, keepdims=True) + EPSILON)


def sigmoid(values):
    return 1.0 / (1.0 + jnp.exp(-values))


def softplus(values):
    return jnp.maximum(values, 0.0) + jnp.log1p(jnp.exp(-jnp.abs(values)))


def spread(columns, first, count):
    rows = columns.shape[0]
    lane = lax.broadcasted_iota(jnp.int32, (rows, LANES), 1)
    tiles = []
    for at in range(first, first + count, 2):
        low = jnp.broadcast_to(columns[:, at : at + 1], (rows, LANES))
        high = jnp.broadcast_to(columns[:, at + 1 : at + 2], (rows, LANES))
        tiles.append(jnp.where(lane < HEAD_DIM, low, high))
    return jnp.concatenate(tiles, axis=1)


def states_kernel(
    shape,
    proj_ref,
    edges_ref,
    taps_ref,
    offset_ref,
    rate_ref,
    signal_ref,
    inward_ref,
    outward_ref,
    within_ref,
    rows_ref,
    block_states_ref,
    block_logs_ref,
    sent_ref,
    padded,
    logs_total,
):
    groups, ratio, content, state_width, heads, shift = shape
    extent = proj_ref.shape[0]
    count = extent // BLOCK
    channels = content + 2 * state_width
    span = ratio * HEAD_DIM
    edge = edges_ref[...].astype(jnp.float32)
    padded[pl.ds(0, 8), :] = jnp.broadcast_to(edge[0:1], (8, channels))
    padded[pl.ds(extent + 8, 8), :] = jnp.broadcast_to(edge[1:2], (8, channels))

    def widen(at, _):
        start = pl.multiple_of(at * BLOCK, BLOCK)
        padded[pl.ds(pl.multiple_of(start + 8, 8), BLOCK), :] = proj_ref[
            pl.ds(start, BLOCK), content : content + channels
        ].astype(jnp.float32)
        return 0

    lax.fori_loop(0, count, widen, 0)
    row = lax.broadcasted_iota(jnp.int32, (BLOCK, BLOCK), 0)
    column = lax.broadcasted_iota(jnp.int32, (BLOCK, BLOCK), 1)
    lower = (row >= column).astype(jnp.float32)
    upper = (row <= column).astype(jnp.float32)
    lane = lax.broadcasted_iota(jnp.int32, (1, LANES), 1)

    def block(at, _):
        start = pl.multiple_of(at * BLOCK, BLOCK)
        here = pl.ds(start, BLOCK)
        filtered = []
        for first in range(0, channels, 2 * LANES):
            part = padded[pl.ds(start, BLOCK + 16), first : first + 2 * LANES]
            taps = taps_ref[:, first : first + 2 * LANES]
            mixed = (
                taps[0:1] * part[7 : 7 + BLOCK]
                + taps[1:2] * part[8 : 8 + BLOCK]
                + taps[2:3] * part[9 : 9 + BLOCK]
            )
            filtered.append((mixed * sigmoid(mixed)).astype(jnp.bfloat16))
        filtered = jnp.concatenate(filtered, axis=1)
        signal = filtered[:, :content]
        inward = filtered[:, content : content + state_width]
        signal_ref[here, :] = signal
        inward_ref[here, :] = inward
        outward_ref[here, :] = filtered[:, content + state_width :]
        raw = proj_ref[here, content + channels :].astype(jnp.float32)
        steps = softplus(raw + offset_ref[...] - shift)
        logs = -steps * rate_ref[...]
        ahead = jnp.dot(lower, logs, precision=HIGHEST, preferred_element_type=jnp.float32)
        behind = jnp.dot(upper, logs, precision=HIGHEST, preferred_element_type=jnp.float32)
        within = jnp.where(lane < heads, ahead, behind)
        final = jnp.where(lane < heads, within[BLOCK - 1 : BLOCK], within[0:1])
        within_ref[here, :] = within
        rows_ref[0 : 2 * heads, here] = within.T[0 : 2 * heads]
        rows_ref[2 * heads : 4 * heads, here] = steps.T[0 : 2 * heads]
        scale = jnp.exp(final - within) * steps
        for group in range(groups):
            wide = signal[:, group * span : (group + 1) * span].astype(jnp.float32)
            scaled = jnp.concatenate(
                [wide * spread(scale, way * heads + group * ratio, ratio) for way in range(2)],
                axis=1,
            ).astype(jnp.bfloat16)
            added = lax.dot_general(
                inward[:, group * STATE : (group + 1) * STATE],
                scaled,
                (((0,), (0,)), ((), ())),
                preferred_element_type=jnp.float32,
            )
            block_states_ref[group, at] = added
            block_logs_ref[group, at] = jnp.concatenate(
                [spread(final, way * heads + group * ratio, ratio) for way in range(2)], axis=1
            )
        return 0

    lax.fori_loop(0, count, block, 0)
    logs_total[...] = jnp.zeros_like(logs_total)
    for group in range(groups):

        def onward(at, state):
            return state * jnp.exp(block_logs_ref[group, at][:, :span]) + block_states_ref[
                group, at
            ][:, :span]

        def back(at, state):
            at = count - 1 - at
            return state * jnp.exp(block_logs_ref[group, at][:, span:]) + block_states_ref[
                group, at
            ][:, span:]

        def total(at, carried):
            return carried + block_logs_ref[group, at]

        empty = jnp.zeros((STATE, span), jnp.float32)
        here = slice(group * STATE, (group + 1) * STATE)
        sent_ref[here, :span] = lax.fori_loop(0, count, onward, empty).astype(jnp.bfloat16)
        sent_ref[here, span:] = lax.fori_loop(0, count, back, empty).astype(jnp.bfloat16)
        decayed = lax.fori_loop(0, count, total, jnp.zeros((1, 2 * span), jnp.float32))
        coarse = decayed.astype(jnp.bfloat16).astype(jnp.float32)
        logs_total[2 * group : 2 * group + 1, :] = coarse
        logs_total[2 * group + 1 : 2 * group + 2, :] = decayed - coarse
    sent_ref[groups * STATE :, :] = logs_total[...].astype(jnp.bfloat16)


def diagonal_kernel(shape, signal_ref, inward_ref, outward_ref, within_ref, rows_ref, result_ref):
    groups, ratio, heads = shape
    count = signal_ref.shape[0] // BLOCK
    row = lax.broadcasted_iota(jnp.int32, (BLOCK, BLOCK), 0)
    column = lax.broadcasted_iota(jnp.int32, (BLOCK, BLOCK), 1)
    lane = lax.broadcasted_iota(jnp.int32, (BLOCK, LANES), 1)

    def block(at, _):
        here = pl.ds(pl.multiple_of(at * BLOCK, BLOCK), BLOCK)
        within = within_ref[here, :]
        for group in range(groups):
            intersect = lax.dot_general(
                outward_ref[here, group * STATE : (group + 1) * STATE],
                inward_ref[here, group * STATE : (group + 1) * STATE],
                (((1,), (1,)), ((), ())),
                preferred_element_type=jnp.float32,
            )
            products = []
            for head in range(group * ratio, (group + 1) * ratio):
                other = heads + head
                gap_ahead = within[:, head : head + 1] - rows_ref[head : head + 1, here]
                gap_behind = within[:, other : other + 1] - rows_ref[other : other + 1, here]
                step_ahead = rows_ref[2 * heads + head : 2 * heads + head + 1, here]
                step_behind = rows_ref[2 * heads + other : 2 * heads + other + 1, here]
                gap = jnp.where(row >= column, gap_ahead, gap_behind)
                step = jnp.where(
                    row > column,
                    step_ahead,
                    jnp.where(row < column, step_behind, step_ahead + step_behind),
                )
                weights = (intersect * jnp.exp(gap) * step).astype(jnp.bfloat16)
                tile = head // 2 * 2 * HEAD_DIM
                products.append(
                    jnp.dot(
                        weights,
                        signal_ref[here, tile : tile + LANES],
                        preferred_element_type=jnp.float32,
                    )
                )
            for pair in range(ratio // 2):
                at_tile = (group * ratio + 2 * pair) * HEAD_DIM
                result_ref[here, at_tile : at_tile + LANES] = jnp.where(
                    lane < HEAD_DIM, products[2 * pair], products[2 * pair + 1]
                )
        return 0

    lax.fori_loop(0, count, block, 0)


def finish_kernel(
    shape,
    gathered_ref,
    block_states_ref,
    block_logs_ref,
    outward_ref,
    within_ref,
    diagonal_ref,
    proj_ref,
    gain_ref,
    mixed_ref,
    total,
):
    groups, ratio, heads = shape
    stretches = gathered_ref.shape[0]
    count = outward_ref.shape[0] // BLOCK
    span = ratio * HEAD_DIM
    me = lax.axis_index("sp")
    for group in range(groups):
        states = slice(group * STATE, (group + 1) * STATE)
        log_at = groups * STATE

        def incoming(source, state, lanes):
            logs = gathered_ref[source, log_at : log_at + 16, lanes].astype(jnp.float32)
            logs = logs[2 * group : 2 * group + 1] + logs[2 * group + 1 : 2 * group + 2]
            return state * jnp.exp(logs) + gathered_ref[source, states, lanes].astype(jnp.float32)

        empty = jnp.zeros((STATE, span), jnp.float32)
        ahead = lax.fori_loop(
            0, me, lambda hop, state: incoming(hop, state, slice(0, span)), empty
        )
        behind = lax.fori_loop(
            0,
            stretches - 1 - me,
            lambda hop, state: incoming(stretches - 1 - hop, state, slice(span, 2 * span)),
            empty,
        )
        wide = slice(group * span, (group + 1) * span)

        def back(hop, state):
            at = count - 1 - hop
            here = pl.ds(pl.multiple_of(at * BLOCK, BLOCK), BLOCK)
            carried = jnp.dot(
                outward_ref[here, states],
                state.astype(jnp.bfloat16),
                preferred_element_type=jnp.float32,
            )
            decay = spread(jnp.exp(within_ref[here, :]), heads + group * ratio, ratio)
            total[here, wide] = diagonal_ref[here, wide] + carried * decay
            return (
                state * jnp.exp(block_logs_ref[group, at][:, span:])
                + block_states_ref[group, at][:, span:]
            )

        lax.fori_loop(0, count, back, behind)

        def onward(at, state):
            here = pl.ds(pl.multiple_of(at * BLOCK, BLOCK), BLOCK)
            carried = jnp.dot(
                outward_ref[here, states],
                state.astype(jnp.bfloat16),
                preferred_element_type=jnp.float32,
            )
            decay = spread(jnp.exp(within_ref[here, :]), group * ratio, ratio)
            gate = proj_ref[here, wide].astype(jnp.float32)
            gated = (total[here, wide] + carried * decay) * (gate * sigmoid(gate))
            scale = lax.rsqrt(jnp.mean(gated * gated, axis=-1, keepdims=True) + EPSILON)
            mixed_ref[here, wide] = (gated * scale * gain_ref[:, wide]).astype(jnp.bfloat16)
            return (
                state * jnp.exp(block_logs_ref[group, at][:, :span])
                + block_states_ref[group, at][:, :span]
            )

        lax.fori_loop(0, count, onward, ahead)


def kernel_call(body, out_shape, scratch, micros):
    return pl.pallas_call(
        body,
        out_shape=out_shape,
        scratch_shapes=scratch,
        cost_estimate=pl.CostEstimate(
            flops=int(micros * 5e8), bytes_accessed=1 << 20, transcendentals=0
        ),
        compiler_params=pltpu.CompilerParams(vmem_limit_bytes=VMEM_LIMIT),
    )


def on_device(
    input_activations,
    norm_gain,
    w_gate,
    w_value,
    w_state_in,
    w_state_out,
    w_step_forward,
    w_step_backward,
    step_offset,
    fading_speed,
    conv_value,
    conv_state_in,
    conv_state_out,
    out_gain,
    w_out,
):
    stretches = lax.axis_size("sp")
    content = w_value.shape[1]
    state_width = w_state_in.shape[1]
    heads = w_step_forward.shape[1]
    groups = state_width // STATE
    ratio = heads // groups
    span = ratio * HEAD_DIM
    channels = content + 2 * state_width
    depth = w_gate.shape[0]
    spare = -2 * heads % LANES

    weights = jnp.concatenate(
        [
            w_gate,
            w_value,
            w_state_in,
            w_state_out,
            w_step_forward,
            w_step_backward,
            jnp.zeros((depth, spare), w_gate.dtype),
        ],
        axis=1,
    )
    all_weights = lax.all_gather(weights, "sp", axis=0, tiled=True)
    normed = (rms_rows(input_activations) * norm_gain).astype(jnp.bfloat16)
    tokens = lax.all_gather(normed, "tp", axis=0, tiled=True)
    proj = jnp.dot(tokens, all_weights, preferred_element_type=jnp.float32).astype(jnp.bfloat16)
    extent = tokens.shape[0]
    count = extent // BLOCK

    onward = [(i, i + 1) for i in range(stretches - 1)]
    back = [(target, source) for source, target in onward]
    low = lax.ppermute(proj[extent - 1 :, content : content + channels], "sp", onward)
    high = lax.ppermute(proj[:1, content : content + channels], "sp", back)
    edges = jnp.concatenate([low, high], axis=0)

    taps = jnp.concatenate([conv_value, conv_state_in, conv_state_out], axis=1)
    padding = ((0, 0), (0, spare))
    offset = jnp.pad(step_offset.reshape(1, 2 * heads), padding)
    rate = jnp.pad(fading_speed.reshape(1, 2 * heads), padding)
    shift = math.log(extent * stretches)

    bf16, f32 = jnp.bfloat16, jnp.float32
    made = jax.ShapeDtypeStruct
    sent_rows = groups * STATE + 16
    signal, inward, outward, within, rows, block_states, block_logs, sent = kernel_call(
        functools.partial(states_kernel, (groups, ratio, content, state_width, heads, shift)),
        (
            made((extent, content), bf16),
            made((extent, state_width), bf16),
            made((extent, state_width), bf16),
            made((extent, LANES), f32),
            made((4 * heads, extent), f32),
            made((groups, count, STATE, 2 * span), f32),
            made((groups, count, 1, 2 * span), f32),
            made((sent_rows, 2 * span), bf16),
        ),
        [pltpu.VMEM((extent + 16, channels), f32), pltpu.VMEM((16, 2 * span), f32)],
        15,
    )(proj, edges, taps, offset, rate)
    gathered = lax.all_gather(sent, "sp")
    diagonal = kernel_call(
        functools.partial(diagonal_kernel, (groups, ratio, heads)),
        made((extent, content), f32),
        [],
        15,
    )(signal, inward, outward, within, rows)
    mixed = kernel_call(
        functools.partial(finish_kernel, (groups, ratio, heads)),
        made((extent, content), bf16),
        [pltpu.VMEM((extent, content), f32)],
        15,
    )(
        gathered,
        block_states,
        block_logs,
        outward,
        within,
        diagonal,
        proj,
        out_gain.reshape(1, content),
    )
    full_out = lax.all_gather(w_out, "sp", axis=1, tiled=True)
    partial = jnp.dot(mixed, full_out, preferred_element_type=jnp.float32).astype(jnp.bfloat16)
    return lax.psum_scatter(partial, "tp", scatter_dimension=0, tiled=True)


def solution(mesh):
    return jax.shard_map(
        on_device,
        mesh=mesh,
        in_specs=(
            P(("sp", "tp"), None),
            P(),
            P("sp", "tp"),
            P("sp", "tp"),
            P("sp", "tp"),
            P("sp", "tp"),
            P("sp", "tp"),
            P("sp", "tp"),
            P(None, "tp"),
            P(None, "tp"),
            P(None, "tp"),
            P(None, "tp"),
            P(None, "tp"),
            P("tp"),
            P("tp", "sp"),
        ),
        out_specs=P(("sp", "tp"), None),
        check_vma=False,
    )
```

time: 543 us -> 347 us (0.64)
  the two profiles are of different devices: /device:TPU:0 before, /device:TPU:12 now
where the time goes in v1:
time: 347 us; the launch traced here: 345 us
  waiting for transfers between devices  264 us (76%)
  Pallas kernels  35.3 us (10%)
  matrix products  17.7 us (5%)
  between operations  13.3 us (4%)
  starting transfers between devices  6.63 us (2%)
  other arithmetic  5.29 us (2%)
    all_gather x1, waiting for transfers between devices, on_device(): all_weights = lax.all_gather(weights, 'sp', axis=0, tiled=True)  105 us
    reduce_scatter x1, waiting for transfers between devices, on_device(): return lax.psum_scatter(partial, 'tp', scatter_dimension=0, tiled=True)  45.3 us
    all_gather x1, waiting for transfers between devices, on_device(): gathered = lax.all_gather(sent, 'sp')  40.4 us
    all_gather x1, waiting for transfers between devices, on_device(): full_out = lax.all_gather(w_out, 'sp', axis=1, tiled=True)  36.2 us
    all_gather x1, waiting for transfers between devices, on_device(): tokens = lax.all_gather(normed, 'tp', axis=0, tiled=True)  34 us
    pallas_call x1, Pallas kernels, on_device(): kernel_call(functools.partial(states_kernel, (groups, ratio, content, sta...  14.2 us
    pallas_call x1, Pallas kernels, on_device(): kernel_call(functools.partial(finish_kernel, (groups, ratio, heads)), mad...  13.3 us
    dot_general x1, matrix products, on_device(): jnp.dot(tokens, all_weights, preferred_element_type=jnp.float32)  11.5 us
  transfers between devices with their start and end apart: 7, of which 6 were waited for; matrix products, arithmetic and copies ran while one was open for 1% of the time, Pallas kernels for 6%

profile of v1, /device:TPU:12, one launch (start us, length us, event | category | flops | bytes accessed | tf_op | source)
XLA Modules:
  0.0 345.1 jit_solution(13361192156153164852)
XLA Ops:
  6.6 0.0 all-gather.6.cloned.1.call-start
  6.6 1.6 fusion
  8.2 2.5 fusion.2
  10.7 0.0 all-gather.6.cloned.1.call-update
  10.7 0.0 all-gather.8.cloned.1.call-start
  10.8 0.1 copy.16
  10.9 0.1 copy.17
  11.1 1.1 concatenate.9
  12.3 0.0 all-gather.12.cloned.1.call-start
  12.3 34.0 %all-gather.6.cloned.1.call-done = bf16[1024,2048]{1,0:T(8,128)(2,1)} async-done(((bf16[256,2048]{1,0:T(8,128)(2,1)}), bf16[1024,2048]{1,0:T(8,128)(2,1)}) %all-gather.6.cloned.1.call-update) | async-done | bytes 4194320 | tf_op jit(solution)/shard_map/all_gather | solution.py:341
  46.3 105.0 %all-gather.8.cloned.1.call-done = bf16[2048,1664]{1,0:T(8,128)(2,1)} async-done(((bf16[256,1664]{1,0:T(8,128)(2,1)}), bf16[2048,1664]{1,0:T(8,128)(2,1)}) %all-gather.8.cloned.1.call-update) | async-done | bytes 6815760 | tf_op jit(solution)/shard_map/all_gather | solution.py:339
  151.3 11.5 %convolution_convert_fusion.1.proj_ref = bf16[1024,1664]{1,0:T(8,128)(2,1)S(1)} fusion(bf16[1024,2048]{1,0:T(8,128)(2,1)} %all-gather.6.cloned.1.call-done, bf16[2048,1664]{1,0:T(8,128)(2,1)} %all-gather.8.cloned.1.call-done), kind=kOutput, calls=%fused_computation.1 | convolution fusion | flops 6981025792 | bytes 14417920 | tf_op jit(solution)/shard_map/dot_general | solution.py:342
  162.9 4.5 %collective-permute-start = (bf16[1,1024]{1,0:T(2,128)(2,1)S(1)}, bf16[1,1024]{1,0:T(2,128)(2,1)S(1)}, u32[]{:S(2)}, u32[]{:S(2)}) collective-permute-start(bf16[1,1024]{1,0:T(2,128)(2,1)S(1)} %get-tuple-element.21), channel_id=1, source_target_pairs={{0,4},{4,8},{8,12},{12,16},{16,20},{20,24},{24,28},{1,5},{5,9},{9,... | collective-permute-start | bytes 6152 | tf_op jit(solution)/shard_map/ppermute | solution.py:348
  167.4 1.9 collective-permute-start.1
  169.3 0.6 pad_maximum_fusion.taps_ref
  169.9 0.1 reshape.18
  170.0 0.1 reshape.19
  170.1 0.6 pad.7.offset_ref
  170.7 0.6 pad.8.rate_ref
  171.3 2.5 collective-permute-done.1
  173.8 0.6 pad_maximum_fusion.1.edges_ref
  174.4 14.2 %shard_map.145 = (bf16[1024,512]{1,0:T(8,128)(2,1)}, bf16[1024,256]{1,0:T(8,128)(2,1)}, bf16[1024,256]{1,0:T(8,128)(2,1)}, f32[1024,128]{1,0:T(8,128)}, f32[32,1...) custom-call(bf16[1024,1664]{1,0:T(8,128)(2,1)} %copy-done.9, ...), custom_call_target="tpu_custom_call" | custom-call | flops 7500000256 | bytes 1048576 | tf_op jit(solution)/shard_map/pallas_call | solution.py:361
  188.6 0.0 all-gather.12.cloned.1.call-update
  188.6 0.0 all-gather.10.cloned.1.call-start
  188.6 0.5 all-gather.10.cloned.1.call-update
  189.2 0.0 reduce-scatter.2.cloned.1.call-start
  189.2 7.9 %shard_map.146.diagonal_ref = f32[1024,512]{1,0:T(8,128)} custom-call(bf16[1024,512]{1,0:T(8,128)(2,1)} %get-tuple-element.18.signal_ref, bf16[1024,256]{1,0:T(8,128)(2,1)} %get-tuple-element.19.inward_ref, bf16[1024,256]{1,0:T(8,128)(2,1)} %get-tuple-element.16.outward_ref, f32[1024,128]{1,0:T(8,128)} %get-tuple-element.17.within_ref, ...), custom_call_target="tpu_custom_call" | custom-call | flops 7500000256 | bytes 1048576 | tf_op jit(solution)/shard_map/pallas_call | solution.py:377
  197.1 40.4 %all-gather.12.cloned.1.call-done = bf16[2176,512]{1,0:T(8,128)(2,1)} async-done(((bf16[272,512]{1,0:T(8,128)(2,1)}), bf16[2176,512]{1,0:T(8,128)(2,1)}) %all-gather.12.cloned.1.call-update) | async-done | bytes 2228240 | tf_op jit(solution)/shard_map/all_gather | solution.py:376
  237.5 13.3 %shard_map.147 = bf16[1024,512]{1,0:T(8,128)(2,1)} custom-call(bf16[8,272,512]{2,1,0:T(8,128)(2,1)} %bitcast.6, f32[2,8,128,512]{3,2,1,0:T(8,128)} %get-tuple-element.14.block_states_ref, f32[2,8,1,512]{3,2,1,0:T(1,128)} %get-tuple-element.15.block_logs_ref, bf16[1024,256]{1,0:T(8,128)(2,1)} %get-tuple-element.16.outward_ref, ...), custom_call_target="tpu_custom_call" | custom-call | flops 7500000256 | bytes 1048576 | tf_op jit(solution)/shard_map/pallas_call | solution.py:383
  250.8 36.2 %all-gather.10.cloned.1.call-done = bf16[512,2048]{1,0:T(8,128)(2,1)} async-done(((bf16[512,256]{1,0:T(8,128)(2,1)}), bf16[512,2048]{1,0:T(8,128)(2,1)}) %all-gather.10.cloned.1.call-update) | async-done | bytes 2097168 | tf_op jit(solution)/shard_map/all_gather | solution.py:398
  287.0 6.2 %convolution_convert_fusion = bf16[1024,2048]{1,0:T(8,128)(2,1)} fusion(bf16[1024,512]{1,0:T(8,128)(2,1)} %shard_map.147, bf16[512,2048]{1,0:T(8,128)(2,1)} %all-gather.10.cloned.1.call-done), kind=kOutput, calls=%fused_computation | convolution fusion | flops 2149580800 | bytes 7340032 | tf_op jit(solution)/shard_map/dot_general | solution.py:399
  293.2 45.3 %reduce-scatter.2.cloned.1.call-done = bf16[256,2048]{1,0:T(8,128)(2,1)} async-done(((bf16[1024,2048]{1,0:T(8,128)(2,1)}), bf16[256,2048]{1,0:T(8,128)(2,1)}) %reduce-scatter.2.cloned.1.call-update) | async-done | bytes 1048592 | tf_op jit(solution)/shard_map/reduce_scatter | solution.py:400
  (30 shorter events, 0.1 us)
Async XLA Ops:
  6.5 4.2 %copy-start.5 = (bf16[256,8]{0,1:T(8,128)(2,1)S(1)}, bf16[256,8]{0,1:T(8,128)(2,1)}, u32[]{:S(2)}) copy-start(bf16[256,8]{0,1:T(8,128)(2,1)} %param.21) | copy-start | bytes 12292
  6.5 4.4 %copy-start.6 = (bf16[256,8]{0,1:T(8,128)(2,1)S(1)}, bf16[256,8]{0,1:T(8,128)(2,1)}, u32[]{:S(2)}) copy-start(bf16[256,8]{0,1:T(8,128)(2,1)} %param.22) | copy-start | bytes 12292
  6.5 4.5 %copy-start = (bf16[256,512]{1,0:T(8,128)(2,1)S(1)}, bf16[256,512]{1,0:T(8,128)(2,1)}, u32[]{:S(2)}) copy-start(bf16[256,512]{1,0:T(8,128)(2,1)} %param.17) | copy-start | bytes 786436
  6.5 4.5 %copy-start.1 = (bf16[256,512]{1,0:T(8,128)(2,1)S(1)}, bf16[256,512]{1,0:T(8,128)(2,1)}, u32[]{:S(2)}) copy-start(bf16[256,512]{1,0:T(8,128)(2,1)} %param.18) | copy-start | bytes 786436
  6.5 4.5 %copy-start.2 = (bf16[256,256]{1,0:T(8,128)(2,1)S(1)}, bf16[256,256]{1,0:T(8,128)(2,1)}, u32[]{:S(2)}) copy-start(bf16[256,256]{1,0:T(8,128)(2,1)} %param.19) | copy-start | bytes 393220
  6.5 4.5 %copy-start.3 = (bf16[256,256]{1,0:T(8,128)(2,1)S(1)}, bf16[256,256]{1,0:T(8,128)(2,1)}, u32[]{:S(2)}) copy-start(bf16[256,256]{1,0:T(8,128)(2,1)} %param.20) | copy-start | bytes 393220
  6.6 39.8 %all-gather.6.cloned.1.call-start = ((), (), s32[]{:S(2)}) async-start(), calls=%async_computation.1 | async-start | bytes 5242880 | tf_op jit(solution)/shard_map/all_gather | solution.py:341
  10.7 140.6 %all-gather.8.cloned.1.call-start = ((), (), s32[]{:S(2)}) async-start(), calls=%async_computation.2 | async-start | bytes 7667712 | tf_op jit(solution)/shard_map/all_gather | solution.py:339
  12.2 157.1 %copy-start.4 = (f32[3,512]{1,0:T(4,128)S(1)}, f32[3,512]{1,0:T(4,128)}, u32[]{:S(2)}) copy-start(f32[3,512]{1,0:T(4,128)} %param.25) | copy-start | bytes 18436
  12.2 157.1 %copy-start.7 = (f32[3,256]{1,0:T(4,128)S(1)}, f32[3,256]{1,0:T(4,128)}, u32[]{:S(2)}) copy-start(f32[3,256]{1,0:T(4,128)} %param.27) | copy-start | bytes 9220
  12.2 157.1 %copy-start.8 = (f32[3,256]{1,0:T(4,128)S(1)}, f32[3,256]{1,0:T(4,128)}, u32[]{:S(2)}) copy-start(f32[3,256]{1,0:T(4,128)} %param.26) | copy-start | bytes 9220
  12.2 157.7 %copy-start.10 = (f32[2,8]{1,0:T(2,128)S(1)}, f32[2,8]{1,0:T(2,128)}, u32[]{:S(2)}) copy-start(f32[2,8]{1,0:T(2,128)} %param.23) | copy-start | bytes 196
  12.3 157.8 %copy-start.11 = (f32[2,8]{1,0:T(2,128)S(1)}, f32[2,8]{1,0:T(2,128)}, u32[]{:S(2)}) copy-start(f32[2,8]{1,0:T(2,128)} %param.24) | copy-start | bytes 196
  12.3 225.2 %all-gather.12.cloned.1.call-start = ((), (), s32[]{:S(2)}) async-start(), calls=%async_computation.5 | async-start | bytes 2506752 | tf_op jit(solution)/shard_map/all_gather | solution.py:376
  162.8 11.5 %copy-start.9 = (bf16[1024,1664]{1,0:T(8,128)(2,1)}, bf16[1024,1664]{1,0:T(8,128)(2,1)S(1)}, u32[]{:S(2)}) copy-start(bf16[1024,1664]{1,0:T(8,128)(2,1)S(1)} %convolution_convert_fusion.1.proj_ref) | copy-start | bytes 10223620
  162.9 8.4 %collective-permute-start = (bf16[1,1024]{1,0:T(2,128)(2,1)S(1)}, bf16[1,1024]{1,0:T(2,128)(2,1)S(1)}, u32[]{:S(2)}, u32[]{:S(2)}) collective-permute-start(bf16[1,1024]{1,0:T(2,128)(2,1)S(1)} %get-tuple-element.21), channel_id=1, source_target_pairs={{0,4},{4,8},{8,12},{12,16},{16,20},{20,24},{24,28},{1,5},{5,9},{9,... | collective-permute-start | bytes 6152 | tf_op jit(solution)/shard_map/ppermute | solution.py:348
  167.4 6.4 %collective-permute-start.1 = (bf16[1,1024]{1,0:T(2,128)(2,1)S(1)}, bf16[1,1024]{1,0:T(2,128)(2,1)S(1)}, u32[]{:S(2)}, u32[]{:S(2)}) collective-permute-start(bf16[1,1024]{1,0:T(2,128)(2,1)S(1)} %get-tuple-element.22), channel_id=1, source_target_pairs={{4,0},{8,4},{12,8},{16,12},{20,16},{24,20},{28,24},{5,1},{9,5},{13... | collective-permute-start | bytes 6152 | tf_op jit(solution)/shard_map/ppermute | solution.py:349
  188.6 98.4 %all-gather.10.cloned.1.call-start = ((), (), s32[]{:S(2)}) async-start(), calls=%async_computation.3 | async-start | bytes 2359296 | tf_op jit(solution)/shard_map/all_gather | solution.py:398
  189.2 149.4 %reduce-scatter.2.cloned.1.call-start = ((), (), s32[]{:S(2)}) async-start(), calls=%async_computation.4 | async-start | bytes 5242880 | tf_op jit(solution)/shard_map/reduce_scatter | solution.py:400
Sparse Core Ops, SparseCore 0:
  10.8 35.4 all-gather.5
  48.5 102.7 all-gather.7
  188.7 48.7 all-gather.11
  239.4 47.5 all-gather.9
  293.3 45.1 reduce-scatter.1

commit v2 on v1

--- a/solution.py
+++ b/solution.py
@@ -150,13 +150,16 @@
 
         empty = jnp.zeros((STATE, span), jnp.float32)
         here = slice(group * STATE, (group + 1) * STATE)
-        sent_ref[here, :span] = lax.fori_loop(0, count, onward, empty).astype(jnp.bfloat16)
-        sent_ref[here, span:] = lax.fori_loop(0, count, back, empty).astype(jnp.bfloat16)
+        sent_ref[0, here, :] = lax.fori_loop(0, count, onward, empty).astype(jnp.bfloat16)
+        sent_ref[1, here, :] = lax.fori_loop(0, count, back, empty).astype(jnp.bfloat16)
         decayed = lax.fori_loop(0, count, total, jnp.zeros((1, 2 * span), jnp.float32))
         coarse = decayed.astype(jnp.bfloat16).astype(jnp.float32)
         logs_total[2 * group : 2 * group + 1, :] = coarse
         logs_total[2 * group + 1 : 2 * group + 2, :] = decayed - coarse
-    sent_ref[groups * STATE :, :] = logs_total[...].astype(jnp.bfloat16)
+    for way in range(2):
+        sent_ref[way, groups * STATE :, :] = logs_total[:, way * span : (way + 1) * span].astype(
+            jnp.bfloat16
+        )
 
 
 def diagonal_kernel(shape, signal_ref, inward_ref, outward_ref, within_ref, rows_ref, result_ref):
@@ -230,19 +233,17 @@
         states = slice(group * STATE, (group + 1) * STATE)
         log_at = groups * STATE
 
-        def incoming(source, state, lanes):
-            logs = gathered_ref[source, log_at : log_at + 16, lanes].astype(jnp.float32)
+        def incoming(source, state):
+            logs = gathered_ref[source, log_at : log_at + 16, :].astype(jnp.float32)
             logs = logs[2 * group : 2 * group + 1] + logs[2 * group + 1 : 2 * group + 2]
-            return state * jnp.exp(logs) + gathered_ref[source, states, lanes].astype(jnp.float32)
+            return state * jnp.exp(logs) + gathered_ref[source, states, :].astype(jnp.float32)
 
         empty = jnp.zeros((STATE, span), jnp.float32)
-        ahead = lax.fori_loop(
-            0, me, lambda hop, state: incoming(hop, state, slice(0, span)), empty
-        )
+        ahead = lax.fori_loop(0, me, incoming, empty)
         behind = lax.fori_loop(
             0,
             stretches - 1 - me,
-            lambda hop, state: incoming(stretches - 1 - hop, state, slice(span, 2 * span)),
+            lambda hop, state: incoming(stretches - 1 - hop, state),
             empty,
         )
         wide = slice(group * span, (group + 1) * span)
@@ -282,6 +283,133 @@
             )
 
         lax.fori_loop(0, count, onward, ahead)
+
+
+def ring_place(index, count):
+    outer, inner = index // 2, index % 2
+    return (1 - inner) * outer + inner * (count - 1 - outer)
+
+
+def ring_index(place, count):
+    far = place // (count // 2)
+    return (1 - far) * (2 * place) + far * (2 * (count - 1 - place) + 1)
+
+
+def greet(peers):
+    barrier = pltpu.get_barrier_semaphore()
+    for peer in peers:
+        pl.semaphore_signal(
+            barrier, inc=1, device_id=peer, device_id_type=pl.DeviceIdType.MESH
+        )
+    pl.semaphore_wait(barrier, len(peers))
+
+
+def remote(source, target, send, receive, peer):
+    return pltpu.make_async_remote_copy(
+        src_ref=source,
+        dst_ref=target,
+        send_sem=send,
+        recv_sem=receive,
+        device_id=peer,
+        device_id_type=pl.DeviceIdType.MESH,
+    )
+
+
+def gather_kernel(
+    stretches,
+    parts,
+    tokens_ref,
+    weights_ref,
+    all_tokens_ref,
+    all_weights_ref,
+    token_send,
+    token_receive,
+    ring_send,
+    ring_receive,
+    own,
+):
+    me, part = lax.axis_index("sp"), lax.axis_index("tp")
+    place = ring_place(me, stretches)
+    half_rows = weights_ref.shape[0] // 2
+    right = (ring_index((place + 1) % stretches, stretches), part)
+    left = (ring_index((place + stretches - 1) % stretches, stretches), part)
+    across = [(me, (part + hop) % parts) for hop in range(1, parts)]
+    greet([right, left] + across)
+    sends = []
+    for hop, peer in enumerate(across):
+        copy = remote(
+            tokens_ref, all_tokens_ref.at[part], token_send.at[hop], token_receive.at[hop], peer
+        )
+        copy.start()
+        sends.append(copy)
+    kept = [
+        pltpu.make_async_copy(tokens_ref, all_tokens_ref.at[part], own.at[0]),
+        pltpu.make_async_copy(weights_ref, all_weights_ref.at[me], own.at[1]),
+    ]
+    ring_sends = []
+    for hop in range(stretches // 2):
+        arriving = []
+        for way, peer in enumerate((right, left)):
+            source = ring_index((place + stretches + (2 * way - 1) * hop) % stretches, stretches)
+            taken = weights_ref if hop == 0 else all_weights_ref.at[source]
+            landed = all_weights_ref.at[source]
+            if hop == stretches // 2 - 1:
+                rows = pl.ds(way * half_rows, half_rows)
+                taken, landed = taken.at[rows], landed.at[rows]
+            copy = remote(
+                taken, landed, ring_send.at[way, hop], ring_receive.at[way, hop], peer
+            )
+            copy.start()
+            arriving.append(copy)
+        if hop == 0:
+            for copy in kept:
+                copy.start()
+        for copy in arriving:
+            copy.wait_recv()
+        ring_sends += arriving
+    for copy in sends:
+        copy.wait()
+    for copy in ring_sends:
+        copy.wait_send()
+    for copy in kept:
+        copy.wait()
+
+
+def exchange_kernel(stretches, sent_ref, gathered_ref, send, receive):
+    me, part = lax.axis_index("sp"), lax.axis_index("tp")
+    peers = [(me + hop) % stretches for hop in range(1, stretches)]
+    greet([(peer, part) for peer in peers])
+    copies = []
+    for hop, peer in enumerate(peers):
+        wrapped = (me + hop + 1) // stretches
+        copy = remote(
+            sent_ref.at[wrapped],
+            gathered_ref.at[me],
+            send.at[hop],
+            receive.at[hop],
+            (peer, part),
+        )
+        copy.start()
+        copies.append(copy)
+    for copy in copies:
+        copy.wait()
+
+
+def remote_call(body, out_shape, inputs, scratch, collective_id):
+    space = pl.BlockSpec(memory_space=pltpu.VMEM)
+    return pl.pallas_call(
+        body,
+        out_shape=out_shape,
+        in_specs=[space] * inputs,
+        out_specs=jax.tree.map(lambda _: space, out_shape),
+        scratch_shapes=scratch,
+        cost_estimate=pl.CostEstimate(
+            flops=int(3e10), bytes_accessed=1 << 20, transcendentals=0
+        ),
+        compiler_params=pltpu.CompilerParams(
+            collective_id=collective_id, has_side_effects=True, vmem_limit_bytes=VMEM_LIMIT
+        ),
+    )
 
 
 def kernel_call(body, out_shape, scratch, micros):
@@ -336,9 +464,29 @@
         ],
         axis=1,
     )
-    all_weights = lax.all_gather(weights, "sp", axis=0, tiled=True)
     normed = (rms_rows(input_activations) * norm_gain).astype(jnp.bfloat16)
-    tokens = lax.all_gather(normed, "tp", axis=0, tiled=True)
+    parts = lax.axis_size("tp")
+    dma = pltpu.SemaphoreType.DMA
+    tokens, all_weights = remote_call(
+        functools.partial(gather_kernel, stretches, parts),
+        (
+            jax.ShapeDtypeStruct((parts, *normed.shape), normed.dtype),
+            jax.ShapeDtypeStruct((stretches, *weights.shape), weights.dtype),
+        ),
+        2,
+        [
+            dma((parts - 1,)),
+            dma((parts - 1,)),
+            dma((2, stretches // 2)),
+            dma((2, stretches // 2)),
+            dma((2,)),
+        ],
+        1,
+    )(normed, weights)
+    tokens, all_weights, w_out = lax.optimization_barrier((tokens, all_weights, w_out))
+    tokens = tokens.reshape(-1, tokens.shape[2])
+    all_weights = all_weights.reshape(-1, all_weights.shape[2])
+    full_out = lax.all_gather(w_out, "sp", axis=1, tiled=True)
     proj = jnp.dot(tokens, all_weights, preferred_element_type=jnp.float32).astype(jnp.bfloat16)
     extent = tokens.shape[0]
     count = extent // BLOCK
@@ -368,12 +516,18 @@
             made((4 * heads, extent), f32),
             made((groups, count, STATE, 2 * span), f32),
             made((groups, count, 1, 2 * span), f32),
-            made((sent_rows, 2 * span), bf16),
+            made((2, sent_rows, span), bf16),
         ),
         [pltpu.VMEM((extent + 16, channels), f32), pltpu.VMEM((16, 2 * span), f32)],
         15,
     )(proj, edges, taps, offset, rate)
-    gathered = lax.all_gather(sent, "sp")
+    gathered = remote_call(
+        functools.partial(exchange_kernel, stretches),
+        made((stretches, sent_rows, span), bf16),
+        1,
+        [dma((stretches - 1,)), dma((stretches - 1,))],
+        2,
+    )(sent)
     diagonal = kernel_call(
         functools.partial(diagonal_kernel, (groups, ratio, heads)),
         made((extent, content), f32),
@@ -395,7 +549,6 @@
         proj,
         out_gain.reshape(1, content),
     )
-    full_out = lax.all_gather(w_out, "sp", axis=1, tiled=True)
     partial = jnp.dot(mixed, full_out, preferred_element_type=jnp.float32).astype(jnp.bfloat16)
     return lax.psum_scatter(partial, "tp", scatter_dimension=0, tiled=True)
 

time: 347 us -> 249 us (0.72)
  waiting for transfers between devices: 264 us -> 46 us
  Pallas kernels: 35.3 us -> 155 us
    all_gather x3 -> x0, waiting for transfers between devices: 179 us -> none  [the longest x1 105 us: on_device(): all_weights = lax.all_gather(weights, 'sp', axis=0, tiled=True)]
    pallas_call x0 -> x2, Pallas kernels: none -> 120 us  [the longest x1 76.8 us: on_device(): remote_call(functools.partial(gather_kernel, stretches, parts), (jax.Shap...]
    all_gather x1, waiting for transfers between devices: 36.2 us -> 0.01 us  [on_device(): full_out = lax.all_gather(w_out, 'sp', axis=1, tiled=True)]
  transfers between devices with their start and end apart: 7 -> 4, of which waited for: 6 -> 2; matrix products, arithmetic and copies ran while one was open for 1% -> 1% of each run, Pallas kernels for 6% -> 32%
where the time goes in v2:
time: 249 us; the launch traced here: 247 us
  Pallas kernels  155 us (62%)
  waiting for transfers between devices  46 us (18%)
  matrix products  17.7 us (7%)
  between operations  13.6 us (5%)
  starting transfers between devices  5.92 us (2%)
  other arithmetic  5.29 us (2%)
  local copies, waits for them, and re-layouts  3.96 us (2%)
    pallas_call x1, Pallas kernels, on_device(): remote_call(functools.partial(gather_kernel, stretches, parts), (jax.Shap...  76.8 us
    reduce_scatter x1, waiting for transfers between devices, on_device(): return lax.psum_scatter(partial, 'tp', scatter_dimension=0, tiled=True)  43.9 us
    pallas_call x1, Pallas kernels, on_device(): remote_call(functools.partial(exchange_kernel, stretches), made((stretche...  43.3 us
    pallas_call x1, Pallas kernels, on_device(): kernel_call(functools.partial(states_kernel, (groups, ratio, content, sta...  14.2 us
    pallas_call x1, Pallas kernels, on_device(): kernel_call(functools.partial(finish_kernel, (groups, ratio, heads)), mad...  13 us
    dot_general x1, matrix products, on_device(): jnp.dot(tokens, all_weights, preferred_element_type=jnp.float32)  11.5 us
    pallas_call x1, Pallas kernels, on_device(): kernel_call(functools.partial(diagonal_kernel, (groups, ratio, heads)), m...  7.79 us
    dot_general x1, matrix products, on_device(): jnp.dot(mixed, full_out, preferred_element_type=jnp.float32)  6.22 us
  transfers between devices with their start and end apart: 4, of which 2 were waited for; matrix products, arithmetic and copies ran while one was open for 1% of the time, Pallas kernels for 32%

profile of v2, /device:TPU:12, one launch (start us, length us, event | category | flops | bytes accessed | tf_op | source)
XLA Modules:
  0.0 247.5 jit_solution(6886488938666576848)
XLA Ops:
  6.5 0.0 all-gather.2.cloned.1.call-start
  6.6 1.6 fusion
  8.2 0.8 copy.16
  9.0 0.8 copy.17
  9.8 2.5 %fusion.2.tokens_ref = bf16[256,2048]{1,0:T(8,128)(2,1)} fusion(bf16[256,2048]{1,0:T(8,128)(2,1)} %param.15, f32[2048]{0:T(1024)} %param.16, f32[256]{0:T(256)S(1)} %add_rsqrt_fusion), kind=kLoop, calls=%fused_computation.6 | loop fusion | flops 2097152 | bytes 2106368 | tf_op jit(solution)/shard_map/convert_element_type | solution.py:467
  12.3 1.1 concatenate.9.weights_ref
  13.4 76.8 %shard_map.145 = (bf16[4,256,2048]{2,1,0:T(8,128)(2,1)}, bf16[8,256,1664]{2,1,0:T(8,128)(2,1)}) custom-call(bf16[256,2048]{1,0:T(8,128)(2,1)} %fusion.2.tokens_ref, bf16[256,1664]{1,0:T(8,128)(2,1)} %concatenate.9.weights_ref), custom_call_target="tpu_custom_call" | custom-call | flops 30000001024 | bytes 1048576 | tf_op jit(solution)/shard_map/pallas_call | solution.py:470
  90.2 0.0 copy-start.4
  90.2 0.0 copy-start.5
  90.3 0.0 copy-start.6
  90.3 0.0 copy-start.8
  90.3 0.0 copy-start.9
  90.3 11.5 %convolution_convert_fusion.1.proj_ref = bf16[1024,1664]{1,0:T(8,128)(2,1)S(1)} fusion(bf16[1024,2048]{1,0:T(8,128)(2,1)} %bitcast.9, bf16[2048,1664]{1,0:T(8,128)(2,1)} %bitcast.8), kind=kOutput, calls=%fused_computation.1 | convolution fusion | flops 6981025792 | bytes 14417920 | tf_op jit(solution)/shard_map/dot_general | solution.py:490
  101.9 3.4 %collective-permute-start = (bf16[1,1024]{1,0:T(2,128)(2,1)S(1)}, bf16[1,1024]{1,0:T(2,128)(2,1)S(1)}, u32[]{:S(2)}, u32[]{:S(2)}) collective-permute-start(bf16[1,1024]{1,0:T(2,128)(2,1)S(1)} %get-tuple-element.31), channel_id=1, source_target_pairs={{0,4},{4,8},{8,12},{12,16},{16,20},{20,24},{24,28},{1,5},{5,9},{9,... | collective-permute-start | bytes 6152 | tf_op jit(solution)/shard_map/ppermute | solution.py:496
  105.2 2.5 collective-permute-start.1
  107.7 0.0 all-gather.2.cloned.1.call-update
  107.7 0.0 reduce-scatter.2.cloned.1.call-start
  107.8 0.6 pad_maximum_fusion.taps_ref
  108.4 0.1 reshape.26
  108.5 0.1 reshape.27
  108.6 0.5 pad.7.offset_ref
  109.1 0.5 pad.8.rate_ref
  109.6 0.0 collective-permute-done
  109.6 2.0 collective-permute-done.1
  111.6 0.6 pad_maximum_fusion.1.edges_ref
  112.2 14.2 %shard_map.146 = (bf16[1024,512]{1,0:T(8,128)(2,1)}, bf16[1024,256]{1,0:T(8,128)(2,1)}, bf16[1024,256]{1,0:T(8,128)(2,1)}, f32[1024,128]{1,0:T(8,128)}, f32[32,1...) custom-call(bf16[1024,1664]{1,0:T(8,128)(2,1)} %copy-done.7, ...), custom_call_target="tpu_custom_call" | custom-call | flops 7500000256 | bytes 1048576 | tf_op jit(solution)/shard_map/pallas_call | solution.py:509
  126.4 7.8 %shard_map.148.diagonal_ref = f32[1024,512]{1,0:T(8,128)} custom-call(bf16[1024,512]{1,0:T(8,128)(2,1)} %get-tuple-element.27.signal_ref, bf16[1024,256]{1,0:T(8,128)(2,1)} %get-tuple-element.28.inward_ref, bf16[1024,256]{1,0:T(8,128)(2,1)} %get-tuple-element.25.outward_ref, f32[1024,128]{1,0:T(8,128)} %get-tuple-element.26.within_ref, ...), custom_call_target="tpu_custom_call" | custom-call | flops 7500000256 | bytes 1048576 | tf_op jit(solution)/shard_map/pallas_call | solution.py:531
  134.2 43.3 %shard_map.147.gathered_ref = bf16[8,272,256]{2,1,0:T(8,128)(2,1)} custom-call(bf16[2,272,256]{2,1,0:T(8,128)(2,1)} %get-tuple-element.22.sent_ref), custom_call_target="tpu_custom_call" | custom-call | flops 30000001024 | bytes 1048576 | tf_op jit(solution)/shard_map/pallas_call | solution.py:524
  177.5 13.0 %shard_map.149 = bf16[1024,512]{1,0:T(8,128)(2,1)} custom-call(bf16[8,272,256]{2,1,0:T(8,128)(2,1)} %shard_map.147.gathered_ref, f32[2,8,128,512]{3,2,1,0:T(8,128)} %get-tuple-element.23.block_states_ref, f32[2,8,1,512]{3,2,1,0:T(1,128)} %get-tuple-element.24.block_logs_ref, bf16[1024,256]{1,0:T(8,128)(2,1)} %get-tuple-element.25.outward_ref, ...), custom_call_target="tpu_custom_call" | custom-call | flops 7500000256 | bytes 1048576 | tf_op jit(solution)/shard_map/pallas_call | solution.py:537
  190.5 6.2 %convolution_convert_fusion = bf16[1024,2048]{1,0:T(8,128)(2,1)} fusion(bf16[1024,512]{1,0:T(8,128)(2,1)} %shard_map.149, bf16[512,2048]{1,0:T(8,128)(2,1)} %all-gather.2.cloned.1.call-done), kind=kOutput, calls=%fused_computation | convolution fusion | flops 2149580800 | bytes 7340032 | tf_op jit(solution)/shard_map/dot_general | solution.py:552
  196.7 0.0 reduce-scatter.2.cloned.1.call-update
  196.7 43.9 %reduce-scatter.2.cloned.1.call-done = bf16[256,2048]{1,0:T(8,128)(2,1)} async-done(((bf16[1024,2048]{1,0:T(8,128)(2,1)}), bf16[256,2048]{1,0:T(8,128)(2,1)}) %reduce-scatter.2.cloned.1.call-update) | async-done | bytes 1048592 | tf_op jit(solution)/shard_map/reduce_scatter | solution.py:553
  (19 shorter events, 0.1 us)
Async XLA Ops:
  6.5 5.8 %copy-start = (bf16[256,512]{1,0:T(8,128)(2,1)S(1)}, bf16[256,512]{1,0:T(8,128)(2,1)}, u32[]{:S(2)}) copy-start(bf16[256,512]{1,0:T(8,128)(2,1)} %param.17) | copy-start | bytes 786436
  6.5 5.8 %copy-start.1 = (bf16[256,512]{1,0:T(8,128)(2,1)S(1)}, bf16[256,512]{1,0:T(8,128)(2,1)}, u32[]{:S(2)}) copy-start(bf16[256,512]{1,0:T(8,128)(2,1)} %param.18) | copy-start | bytes 786436
  6.5 5.8 %copy-start.2 = (bf16[256,256]{1,0:T(8,128)(2,1)S(1)}, bf16[256,256]{1,0:T(8,128)(2,1)}, u32[]{:S(2)}) copy-start(bf16[256,256]{1,0:T(8,128)(2,1)} %param.19) | copy-start | bytes 393220
  6.5 5.8 %copy-start.3 = (bf16[256,256]{1,0:T(8,128)(2,1)S(1)}, bf16[256,256]{1,0:T(8,128)(2,1)}, u32[]{:S(2)}) copy-start(bf16[256,256]{1,0:T(8,128)(2,1)} %param.20) | copy-start | bytes 393220
  6.5 183.9 %all-gather.2.cloned.1.call-start = ((), (), s32[]{:S(2)}) async-start(), calls=%async_computation.1 | async-start | bytes 2359296 | tf_op jit(solution)/shard_map/all_gather | solution.py:489
  90.2 17.6 %copy-start.4 = (f32[3,512]{1,0:T(4,128)S(1)}, f32[3,512]{1,0:T(4,128)}, u32[]{:S(2)}) copy-start(f32[3,512]{1,0:T(4,128)} %param.25) | copy-start | bytes 18436
  90.2 17.6 %copy-start.5 = (f32[3,256]{1,0:T(4,128)S(1)}, f32[3,256]{1,0:T(4,128)}, u32[]{:S(2)}) copy-start(f32[3,256]{1,0:T(4,128)} %param.27) | copy-start | bytes 9220
  90.3 17.6 %copy-start.6 = (f32[3,256]{1,0:T(4,128)S(1)}, f32[3,256]{1,0:T(4,128)}, u32[]{:S(2)}) copy-start(f32[3,256]{1,0:T(4,128)} %param.26) | copy-start | bytes 9220
  90.3 18.2 %copy-start.8 = (f32[2,8]{1,0:T(2,128)S(1)}, f32[2,8]{1,0:T(2,128)}, u32[]{:S(2)}) copy-start(f32[2,8]{1,0:T(2,128)} %param.23) | copy-start | bytes 196
  90.3 18.2 %copy-start.9 = (f32[2,8]{1,0:T(2,128)S(1)}, f32[2,8]{1,0:T(2,128)}, u32[]{:S(2)}) copy-start(f32[2,8]{1,0:T(2,128)} %param.24) | copy-start | bytes 196
  101.8 10.4 %copy-start.7 = (bf16[1024,1664]{1,0:T(8,128)(2,1)}, bf16[1024,1664]{1,0:T(8,128)(2,1)S(1)}, u32[]{:S(2)}) copy-start(bf16[1024,1664]{1,0:T(8,128)(2,1)S(1)} %convolution_convert_fusion.1.proj_ref) | copy-start | bytes 10223620
  101.9 7.8 %collective-permute-start = (bf16[1,1024]{1,0:T(2,128)(2,1)S(1)}, bf16[1,1024]{1,0:T(2,128)(2,1)S(1)}, u32[]{:S(2)}, u32[]{:S(2)}) collective-permute-start(bf16[1,1024]{1,0:T(2,128)(2,1)S(1)} %get-tuple-element.31), channel_id=1, source_target_pairs={{0,4},{4,8},{8,12},{12,16},{16,20},{20,24},{24,28},{1,5},{5,9},{9,... | collective-permute-start | bytes 6152 | tf_op jit(solution)/shard_map/ppermute | solution.py:496
  105.2 6.4 %collective-permute-start.1 = (bf16[1,1024]{1,0:T(2,128)(2,1)S(1)}, bf16[1,1024]{1,0:T(2,128)(2,1)S(1)}, u32[]{:S(2)}, u32[]{:S(2)}) collective-permute-start(bf16[1,1024]{1,0:T(2,128)(2,1)S(1)} %get-tuple-element.32), channel_id=1, source_target_pairs={{4,0},{8,4},{12,8},{16,12},{20,16},{24,20},{28,24},{5,1},{9,5},{13... | collective-permute-start | bytes 6152 | tf_op jit(solution)/shard_map/ppermute | solution.py:497
  107.7 132.9 %reduce-scatter.2.cloned.1.call-start = ((), (), s32[]{:S(2)}) async-start(), calls=%async_computation.2 | async-start | bytes 5242880 | tf_op jit(solution)/shard_map/reduce_scatter | solution.py:553
Sparse Core Ops, SparseCore 0:
  107.9 65.4 all-gather.1
  196.8 43.7 reduce-scatter.1

commit v3 on v2

--- a/solution.py
+++ b/solution.py
@@ -375,7 +375,20 @@
         copy.wait()
 
 
-def exchange_kernel(stretches, sent_ref, gathered_ref, send, receive):
+def exchange_kernel(
+    stretches,
+    shape,
+    sent_ref,
+    signal_ref,
+    inward_ref,
+    outward_ref,
+    within_ref,
+    rows_ref,
+    gathered_ref,
+    result_ref,
+    send,
+    receive,
+):
     me, part = lax.axis_index("sp"), lax.axis_index("tp")
     peers = [(me + hop) % stretches for hop in range(1, stretches)]
     greet([(peer, part) for peer in peers])
@@ -391,8 +404,111 @@
         )
         copy.start()
         copies.append(copy)
+    diagonal_kernel(
+        shape, signal_ref, inward_ref, outward_ref, within_ref, rows_ref, result_ref
+    )
     for copy in copies:
         copy.wait()
+
+
+def output_kernel(
+    mixed_ref,
+    weights_ref,
+    result_ref,
+    near_out,
+    near_in,
+    far_out,
+    far_in,
+    own,
+    near_send,
+    near_receive,
+    far_send,
+    far_receive,
+):
+    me, part = lax.axis_index("sp"), lax.axis_index("tp")
+    pair, place = part // 2, part % 2
+    near = (me, 2 * pair + 1 - place)
+    far = (me, 2 * (1 - pair) + place)
+    greet([near, far])
+    extent = result_ref.shape[0]
+    piece = extent // 2
+    width = 4 * LANES
+
+    def product(block, at, store):
+        start = pl.multiple_of(block * extent + at * piece, piece)
+        rows = mixed_ref[pl.ds(start, piece), :]
+
+        def tile(step, _):
+            columns = pl.ds(pl.multiple_of(step * width, width), width)
+            total = jnp.dot(rows, weights_ref[:, columns], preferred_element_type=jnp.float32)
+            store(columns, total)
+            return 0
+
+        lax.fori_loop(0, result_ref.shape[1] // width, tile, 0)
+
+    def rows_of(at):
+        return pl.ds(at * piece, piece)
+
+    def to_near(block, turn, at):
+        def store(columns, total):
+            near_out[turn, rows_of(at), columns] = total.astype(jnp.bfloat16)
+
+        product(block, at, store)
+        return remote(
+            near_out.at[turn, rows_of(at)],
+            near_in.at[turn, rows_of(at)],
+            near_send.at[turn, at],
+            near_receive.at[turn, at],
+            near,
+        )
+
+    def to_far(block, at, arriving):
+        arriving.wait_recv()
+
+        def store(columns, total):
+            total = total + near_in[0, rows_of(at), columns].astype(jnp.float32)
+            far_out[rows_of(at), columns] = total.astype(jnp.bfloat16)
+
+        product(block, at, store)
+        return remote(
+            far_out.at[rows_of(at)],
+            far_in.at[rows_of(at)],
+            far_send.at[at],
+            far_receive.at[at],
+            far,
+        )
+
+    def keep(at):
+        def store(columns, total):
+            own[rows_of(at), columns] = total
+
+        product(part, at, store)
+
+    theirs, mine = 2 * (1 - pair) + 1 - place, 2 * (1 - pair) + place
+    first = [to_near(theirs, 0, 0), None]
+    first[1] = to_near(theirs, 0, 1)
+    first[0].start()
+    keep(0)
+    first[1].start()
+    keep(1)
+    across = [to_far(mine, 0, first[0]), None]
+    across[1] = to_far(mine, 1, first[1])
+    across[0].start()
+    second = [to_near(2 * pair + 1 - place, 1, 0), None]
+    across[1].start()
+    second[1] = to_near(2 * pair + 1 - place, 1, 1)
+    second[0].start()
+    second[0].wait_recv()
+    own[rows_of(0), :] += near_in[1, rows_of(0), :].astype(jnp.float32)
+    second[1].start()
+    second[1].wait_recv()
+    own[rows_of(1), :] += near_in[1, rows_of(1), :].astype(jnp.float32)
+    for at in range(2):
+        across[at].wait_recv()
+        total = own[rows_of(at), :] + far_in[rows_of(at), :].astype(jnp.float32)
+        result_ref[rows_of(at), :] = total.astype(result_ref.dtype)
+    for copy in first + second + across:
+        copy.wait_send()
 
 
 def remote_call(body, out_shape, inputs, scratch, collective_id):
@@ -521,19 +637,13 @@
         [pltpu.VMEM((extent + 16, channels), f32), pltpu.VMEM((16, 2 * span), f32)],
         15,
     )(proj, edges, taps, offset, rate)
-    gathered = remote_call(
-        functools.partial(exchange_kernel, stretches),
-        made((stretches, sent_rows, span), bf16),
-        1,
+    gathered, diagonal = remote_call(
+        functools.partial(exchange_kernel, stretches, (groups, ratio, heads)),
+        (made((stretches, sent_rows, span), bf16), made((extent, content), f32)),
+        6,
         [dma((stretches - 1,)), dma((stretches - 1,))],
         2,
-    )(sent)
-    diagonal = kernel_call(
-        functools.partial(diagonal_kernel, (groups, ratio, heads)),
-        made((extent, content), f32),
-        [],
-        15,
-    )(signal, inward, outward, within, rows)
+    )(sent, signal, inward, outward, within, rows)
     mixed = kernel_call(
         functools.partial(finish_kernel, (groups, ratio, heads)),
         made((extent, content), bf16),
@@ -549,8 +659,27 @@
         proj,
         out_gain.reshape(1, content),
     )
-    partial = jnp.dot(mixed, full_out, preferred_element_type=jnp.float32).astype(jnp.bfloat16)
-    return lax.psum_scatter(partial, "tp", scatter_dimension=0, tiled=True)
+    rows_out, features = input_activations.shape
+    if parts != 4:
+        partial = jnp.dot(mixed, full_out, preferred_element_type=f32).astype(bf16)
+        return lax.psum_scatter(partial, "tp", scatter_dimension=0, tiled=True)
+    return remote_call(
+        output_kernel,
+        made((rows_out, features), bf16),
+        2,
+        [
+            pltpu.VMEM((2, rows_out, features), bf16),
+            pltpu.VMEM((2, rows_out, features), bf16),
+            pltpu.VMEM((rows_out, features), bf16),
+            pltpu.VMEM((rows_out, features), bf16),
+            pltpu.VMEM((rows_out, features), f32),
+            dma((2, 2)),
+            dma((2, 2)),
+            dma((2,)),
+            dma((2,)),
+        ],
+        3,
+    )(mixed, full_out)
 
 
 def solution(mesh):

time: 249 us -> 226 us (0.908)
  waiting for transfers between devices: 46 us -> 2.02 us
  Pallas kernels: 155 us -> 182 us
  matrix products: 17.7 us -> 11.5 us
    reduce_scatter x1 -> x0, waiting for transfers between devices: 43.9 us -> none  [on_device(): return lax.psum_scatter(partial, 'tp', scatter_dimension=0, tiled=True)]
    pallas_call x2, Pallas kernels: 51.1 us -> 77.5 us  [the longest x1 43.3 us: on_device(): remote_call(functools.partial(exchange_kernel, stretches, (groups, ratio,...]
    dot_general x1 -> x0, matrix products: 6.22 us -> none  [on_device(): jnp.dot(mixed, full_out, preferred_element_type=jnp.float32)]
  transfers between devices with their start and end apart: 4 -> 3, of which waited for: 2 -> 1; matrix products, arithmetic and copies ran while one was open for 1% -> 1% of each run, Pallas kernels for 32% -> 31%
where the time goes in v3:
time: 226 us
  Pallas kernels  182 us (81%)
  between operations  13.6 us (6%)
  matrix products  11.5 us (5%)
  local copies, waits for them, and re-layouts  6.33 us (3%)
  starting transfers between devices  5.88 us (3%)
  other arithmetic  5.29 us (2%)
    pallas_call x1, Pallas kernels, on_device(): remote_call(functools.partial(gather_kernel, stretches, parts), (jax.Shap...  76.8 us
    pallas_call x1, Pallas kernels, on_device(): remote_call(functools.partial(exchange_kernel, stretches, (groups, ratio,...  43.3 us
    pallas_call x1, Pallas kernels, on_device(): remote_call(output_kernel, made((rows_out, features), bf16), 2, [pltpu.VM...  34.2 us
    pallas_call x1, Pallas kernels, on_device(): kernel_call(functools.partial(states_kernel, (groups, ratio, content, sta...  14.2 us
    pallas_call x1, Pallas kernels, on_device(): kernel_call(functools.partial(finish_kernel, (groups, ratio, heads)), mad...  13 us
    dot_general x1, matrix products, on_device(): jnp.dot(tokens, all_weights, preferred_element_type=jnp.float32)  11.5 us
  transfers between devices with their start and end apart: 3, of which 1 were waited for; matrix products, arithmetic and copies ran while one was open for 1% of the time, Pallas kernels for 31%

profile of v3, /device:TPU:12, one launch (start us, length us, event | category | flops | bytes accessed | tf_op | source)
XLA Modules:
  0.0 226.1 jit_solution(3562685345439508025)
XLA Ops:
  6.5 0.0 all-gather.2.cloned.1.call-start
  6.6 1.6 fusion
  8.2 0.8 copy.16
  9.0 0.8 copy.17
  9.8 2.5 %fusion.2.tokens_ref = bf16[256,2048]{1,0:T(8,128)(2,1)} fusion(bf16[256,2048]{1,0:T(8,128)(2,1)} %param.15, f32[2048]{0:T(1024)} %param.16, f32[256]{0:T(256)S(1)} %add_rsqrt_fusion), kind=kLoop, calls=%fused_computation.5 | loop fusion | flops 2097152 | bytes 2106368 | tf_op jit(solution)/shard_map/convert_element_type | solution.py:583
  12.3 0.0 copy-done
  12.3 1.1 concatenate.9.weights_ref
  13.4 76.8 %shard_map.145 = (bf16[4,256,2048]{2,1,0:T(8,128)(2,1)}, bf16[8,256,1664]{2,1,0:T(8,128)(2,1)}) custom-call(bf16[256,2048]{1,0:T(8,128)(2,1)} %fusion.2.tokens_ref, bf16[256,1664]{1,0:T(8,128)(2,1)} %concatenate.9.weights_ref), custom_call_target="tpu_custom_call" | custom-call | flops 30000001024 | bytes 1048576 | tf_op jit(solution)/shard_map/pallas_call | solution.py:586
  90.2 0.0 copy-start.4
  90.3 0.0 copy-start.5
  90.3 0.0 copy-start.6
  90.3 0.0 copy-start.8
  90.3 0.0 copy-start.9
  90.3 11.5 %convolution_convert_fusion.proj_ref = bf16[1024,1664]{1,0:T(8,128)(2,1)S(1)} fusion(bf16[1024,2048]{1,0:T(8,128)(2,1)} %bitcast.7, bf16[2048,1664]{1,0:T(8,128)(2,1)} %bitcast.6), kind=kOutput, calls=%fused_computation | convolution fusion | flops 6981025792 | bytes 14417920 | tf_op jit(solution)/shard_map/dot_general | solution.py:606
  101.8 0.0 copy-start.7
  101.9 3.4 %collective-permute-start = (bf16[1,1024]{1,0:T(2,128)(2,1)S(1)}, bf16[1,1024]{1,0:T(2,128)(2,1)S(1)}, u32[]{:S(2)}, u32[]{:S(2)}) collective-permute-start(bf16[1,1024]{1,0:T(2,128)(2,1)S(1)} %get-tuple-element.35), channel_id=1, source_target_pairs={{0,4},{4,8},{8,12},{12,16},{16,20},{20,24},{24,28},{1,5},{5,9},{9,... | collective-permute-start | bytes 6152 | tf_op jit(solution)/shard_map/ppermute | solution.py:612
  105.2 2.5 %collective-permute-start.1 = (bf16[1,1024]{1,0:T(2,128)(2,1)S(1)}, bf16[1,1024]{1,0:T(2,128)(2,1)S(1)}, u32[]{:S(2)}, u32[]{:S(2)}) collective-permute-start(bf16[1,1024]{1,0:T(2,128)(2,1)S(1)} %get-tuple-element.36), channel_id=1, source_target_pairs={{4,0},{8,4},{12,8},{16,12},{20,16},{24,20},{28,24},{5,1},{9,5},{13... | collective-permute-start | bytes 6152 | tf_op jit(solution)/shard_map/ppermute | solution.py:613
  107.7 0.0 all-gather.2.cloned.1.call-update
  107.8 0.6 pad_maximum_fusion.taps_ref
  108.4 0.1 reshape.26
  108.5 0.0 copy-done.9
  108.5 0.1 reshape.27
  108.5 0.5 pad.7.offset_ref
  109.1 0.6 pad.8.rate_ref
  109.6 0.0 collective-permute-done
  109.6 2.0 collective-permute-done.1
  111.6 0.6 pad_maximum_fusion.1.edges_ref
  112.2 14.2 %shard_map.146 = (bf16[1024,512]{1,0:T(8,128)(2,1)}, bf16[1024,256]{1,0:T(8,128)(2,1)}, bf16[1024,256]{1,0:T(8,128)(2,1)}, f32[1024,128]{1,0:T(8,128)}, f32[32,1...) custom-call(bf16[1024,1664]{1,0:T(8,128)(2,1)} %copy-done.7, ...), custom_call_target="tpu_custom_call" | custom-call | flops 7500000256 | bytes 1048576 | tf_op jit(solution)/shard_map/pallas_call | solution.py:625
  126.5 43.3 %shard_map.147 = (bf16[8,272,256]{2,1,0:T(8,128)(2,1)}, f32[1024,512]{1,0:T(8,128)}) custom-call(bf16[2,272,256]{2,1,0:T(8,128)(2,1)} %get-tuple-element.24.sent_ref, bf16[1024,512]{1,0:T(8,128)(2,1)} %get-tuple-element.25.signal_ref, bf16[1024,256]{1,0:T(8,128)(2,1)} %get-tuple-element.26.inward_ref, bf16[1024,256]{1,0:T(8,128)(2,1)} %get-tuple-element.27.outward_ref, ...), custom_call_target="tpu_custom_call" | custom-call | flops 30000001024 | bytes 1048576 | tf_op jit(solution)/shard_map/pallas_call | solution.py:640
  169.8 13.0 %shard_map.148.mixed_ref = bf16[1024,512]{1,0:T(8,128)(2,1)} custom-call(bf16[8,272,256]{2,1,0:T(8,128)(2,1)} %get-tuple-element.30.gathered_ref, f32[2,8,128,512]{3,2,1,0:T(8,128)} %get-tuple-element.31.block_states_ref, f32[2,8,1,512]{3,2,1,0:T(1,128)} %get-tuple-element.32.block_logs_ref, bf16[1024,256]{1,0:T(8,128)(2,1)} %get-tuple-element.27.outward_ref, ...), custom_call_target="tpu_custom_call" | custom-call | flops 7500000256 | bytes 1048576 | tf_op jit(solution)/shard_map/pallas_call | solution.py:647
  182.8 34.2 %shard_map.149 = bf16[256,2048]{1,0:T(8,128)(2,1)} custom-call(bf16[1024,512]{1,0:T(8,128)(2,1)} %shard_map.148.mixed_ref, bf16[512,2048]{1,0:T(8,128)(2,1)} %all-gather.2.cloned.1.call-done.weights_ref), custom_call_target="tpu_custom_call" | custom-call | flops 30000001024 | bytes 1048576 | tf_op jit(solution)/shard_map/pallas_call | solution.py:666
  217.0 2.3 %copy.19 = bf16[256,2048]{1,0:T(8,128)(2,1)} copy(bf16[256,2048]{1,0:T(8,128)(2,1)} %shard_map.149) | data formatting | bytes 2097152
  (16 shorter events, 0.1 us)
Async XLA Ops:
  6.5 5.8 %copy-start = (bf16[256,512]{1,0:T(8,128)(2,1)S(1)}, bf16[256,512]{1,0:T(8,128)(2,1)}, u32[]{:S(2)}) copy-start(bf16[256,512]{1,0:T(8,128)(2,1)} %param.17) | copy-start | bytes 786436
  6.5 5.8 %copy-start.1 = (bf16[256,512]{1,0:T(8,128)(2,1)S(1)}, bf16[256,512]{1,0:T(8,128)(2,1)}, u32[]{:S(2)}) copy-start(bf16[256,512]{1,0:T(8,128)(2,1)} %param.18) | copy-start | bytes 786436
  6.5 5.8 %copy-start.2 = (bf16[256,256]{1,0:T(8,128)(2,1)S(1)}, bf16[256,256]{1,0:T(8,128)(2,1)}, u32[]{:S(2)}) copy-start(bf16[256,256]{1,0:T(8,128)(2,1)} %param.19) | copy-start | bytes 393220
  6.5 5.8 %copy-start.3 = (bf16[256,256]{1,0:T(8,128)(2,1)S(1)}, bf16[256,256]{1,0:T(8,128)(2,1)}, u32[]{:S(2)}) copy-start(bf16[256,256]{1,0:T(8,128)(2,1)} %param.20) | copy-start | bytes 393220
  6.5 176.2 %all-gather.2.cloned.1.call-start = ((), (), s32[]{:S(2)}) async-start(), calls=%async_computation | async-start | bytes 2359296 | tf_op jit(solution)/shard_map/all_gather | solution.py:605
  90.2 17.5 %copy-start.4 = (f32[3,512]{1,0:T(4,128)S(1)}, f32[3,512]{1,0:T(4,128)}, u32[]{:S(2)}) copy-start(f32[3,512]{1,0:T(4,128)} %param.25) | copy-start | bytes 18436
  90.3 17.5 %copy-start.5 = (f32[3,256]{1,0:T(4,128)S(1)}, f32[3,256]{1,0:T(4,128)}, u32[]{:S(2)}) copy-start(f32[3,256]{1,0:T(4,128)} %param.27) | copy-start | bytes 9220
  90.3 17.5 %copy-start.6 = (f32[3,256]{1,0:T(4,128)S(1)}, f32[3,256]{1,0:T(4,128)}, u32[]{:S(2)}) copy-start(f32[3,256]{1,0:T(4,128)} %param.26) | copy-start | bytes 9220
  90.3 18.1 %copy-start.8 = (f32[2,8]{1,0:T(2,128)S(1)}, f32[2,8]{1,0:T(2,128)}, u32[]{:S(2)}) copy-start(f32[2,8]{1,0:T(2,128)} %param.23) | copy-start | bytes 196
  90.3 18.2 %copy-start.9 = (f32[2,8]{1,0:T(2,128)S(1)}, f32[2,8]{1,0:T(2,128)}, u32[]{:S(2)}) copy-start(f32[2,8]{1,0:T(2,128)} %param.24) | copy-start | bytes 196
  101.8 10.4 %copy-start.7 = (bf16[1024,1664]{1,0:T(8,128)(2,1)}, bf16[1024,1664]{1,0:T(8,128)(2,1)S(1)}, u32[]{:S(2)}) copy-start(bf16[1024,1664]{1,0:T(8,128)(2,1)S(1)} %convolution_convert_fusion.proj_ref) | copy-start | bytes 10223620
  101.9 7.8 %collective-permute-start = (bf16[1,1024]{1,0:T(2,128)(2,1)S(1)}, bf16[1,1024]{1,0:T(2,128)(2,1)S(1)}, u32[]{:S(2)}, u32[]{:S(2)}) collective-permute-start(bf16[1,1024]{1,0:T(2,128)(2,1)S(1)} %get-tuple-element.35), channel_id=1, source_target_pairs={{0,4},{4,8},{8,12},{12,16},{16,20},{20,24},{24,28},{1,5},{5,9},{9,... | collective-permute-start | bytes 6152 | tf_op jit(solution)/shard_map/ppermute | solution.py:612
  105.2 6.4 %collective-permute-start.1 = (bf16[1,1024]{1,0:T(2,128)(2,1)S(1)}, bf16[1,1024]{1,0:T(2,128)(2,1)S(1)}, u32[]{:S(2)}, u32[]{:S(2)}) collective-permute-start(bf16[1,1024]{1,0:T(2,128)(2,1)S(1)} %get-tuple-element.36), channel_id=1, source_target_pairs={{4,0},{8,4},{12,8},{16,12},{20,16},{24,20},{28,24},{5,1},{9,5},{13... | collective-permute-start | bytes 6152 | tf_op jit(solution)/shard_map/ppermute | solution.py:613
Sparse Core Ops, SparseCore 0:
  107.9 61.3 all-gather.1

commit v4 on v3

--- a/solution.py
+++ b/solution.py
@@ -64,9 +64,11 @@
     count = extent // BLOCK
     channels = content + 2 * state_width
     span = ratio * HEAD_DIM
-    edge = edges_ref[...].astype(jnp.float32)
-    padded[pl.ds(0, 8), :] = jnp.broadcast_to(edge[0:1], (8, channels))
-    padded[pl.ds(extent + 8, 8), :] = jnp.broadcast_to(edge[1:2], (8, channels))
+    me, last = lax.axis_index("sp"), lax.axis_size("sp") - 1
+    low = edges_ref[0, :, content : content + channels].astype(jnp.float32)
+    high = edges_ref[1, :, content : content + channels].astype(jnp.float32)
+    padded[pl.ds(0, 8), :] = jnp.where(me > 0, low[8:], 0.0)
+    padded[pl.ds(extent + 8, 8), :] = jnp.where(me < last, high[:8], 0.0)
 
     def widen(at, _):
         start = pl.multiple_of(at * BLOCK, BLOCK)
@@ -320,8 +322,14 @@
     parts,
     tokens_ref,
     weights_ref,
+    proj_ref,
+    edges_ref,
     all_tokens_ref,
     all_weights_ref,
+    sums,
+    edge_out,
+    edge_send,
+    edge_receive,
     token_send,
     token_receive,
     ring_send,
@@ -334,7 +342,39 @@
     right = (ring_index((place + 1) % stretches, stretches), part)
     left = (ring_index((place + stretches - 1) % stretches, stretches), part)
     across = [(me, (part + hop) % parts) for hop in range(1, parts)]
-    greet([right, left] + across)
+    after = ((me + 1) % stretches, part)
+    before = ((me + stretches - 1) % stretches, part)
+    greet([right, left, after, before] + across)
+    rows, depth = tokens_ref.shape[0], weights_ref.shape[0]
+    columns = weights_ref.shape[1]
+
+    def project(sources, fresh, final):
+        def one(at, _):
+            here = pl.ds(pl.multiple_of(at * rows, rows), rows)
+            for first in range(0, columns, 2 * LANES):
+                tile = slice(first, min(first + 2 * LANES, columns))
+                total = None
+                for source in sources:
+                    if isinstance(source, int):
+                        taken = slice(source * depth, (source + 1) * depth)
+                    else:
+                        taken = pl.ds(pl.multiple_of(source * depth, LANES), depth)
+                    term = jnp.dot(
+                        all_tokens_ref[at, :, taken],
+                        all_weights_ref[source, :, tile],
+                        preferred_element_type=jnp.float32,
+                    )
+                    total = term if total is None else total + term
+                if not fresh:
+                    total = total + sums[here, tile]
+                if final:
+                    proj_ref[here, tile] = total.astype(proj_ref.dtype)
+                else:
+                    sums[here, tile] = total
+            return 0
+
+        lax.fori_loop(0, parts, one, 0)
+
     sends = []
     for hop, peer in enumerate(across):
         copy = remote(
@@ -354,8 +394,8 @@
             taken = weights_ref if hop == 0 else all_weights_ref.at[source]
             landed = all_weights_ref.at[source]
             if hop == stretches // 2 - 1:
-                rows = pl.ds(way * half_rows, half_rows)
-                taken, landed = taken.at[rows], landed.at[rows]
+                piece = pl.ds(way * half_rows, half_rows)
+                taken, landed = taken.at[piece], landed.at[piece]
             copy = remote(
                 taken, landed, ring_send.at[way, hop], ring_receive.at[way, hop], peer
             )
@@ -364,14 +404,38 @@
         if hop == 0:
             for copy in kept:
                 copy.start()
+        if hop == stretches // 2 - 1:
+            for copy in sends:
+                copy.wait()
+            for copy in kept:
+                copy.wait()
+            if depth % LANES == 0:
+                near = [
+                    ring_index((place + stretches + away) % stretches, stretches)
+                    for away in range(-hop, hop + 1)
+                ]
+                near[hop] = me
+                project(near, True, False)
         for copy in arriving:
             copy.wait_recv()
         ring_sends += arriving
-    for copy in sends:
-        copy.wait()
+    if depth % LANES == 0:
+        opposite = ring_index((place + stretches // 2) % stretches, stretches)
+        project([opposite], False, True)
+    else:
+        project(list(range(stretches)), True, True)
+    extent = parts * rows
+    edge_out[0] = proj_ref[pl.ds(extent - 16, 16), :]
+    edge_out[1] = proj_ref[pl.ds(0, 16), :]
     for copy in ring_sends:
         copy.wait_send()
-    for copy in kept:
+    edges = [
+        remote(edge_out.at[way], edges_ref.at[way], edge_send.at[way], edge_receive.at[way], peer)
+        for way, peer in enumerate((after, before))
+    ]
+    for copy in edges:
+        copy.start()
+    for copy in edges:
         copy.wait()
 
 
@@ -583,14 +647,24 @@
     normed = (rms_rows(input_activations) * norm_gain).astype(jnp.bfloat16)
     parts = lax.axis_size("tp")
     dma = pltpu.SemaphoreType.DMA
-    tokens, all_weights = remote_call(
+    rows_here, features = normed.shape
+    extent = parts * rows_here
+    count = extent // BLOCK
+    wide = weights.shape[1]
+    proj, edges = remote_call(
         functools.partial(gather_kernel, stretches, parts),
         (
-            jax.ShapeDtypeStruct((parts, *normed.shape), normed.dtype),
-            jax.ShapeDtypeStruct((stretches, *weights.shape), weights.dtype),
+            jax.ShapeDtypeStruct((extent, wide), normed.dtype),
+            jax.ShapeDtypeStruct((2, 16, wide), normed.dtype),
         ),
         2,
         [
+            pltpu.VMEM((parts, rows_here, features), normed.dtype),
+            pltpu.VMEM((stretches, depth, wide), weights.dtype),
+            pltpu.VMEM((extent, wide), jnp.float32),
+            pltpu.VMEM((2, 16, wide), normed.dtype),
+            dma((2,)),
+            dma((2,)),
             dma((parts - 1,)),
             dma((parts - 1,)),
             dma((2, stretches // 2)),
@@ -599,19 +673,8 @@
         ],
         1,
     )(normed, weights)
-    tokens, all_weights, w_out = lax.optimization_barrier((tokens, all_weights, w_out))
-    tokens = tokens.reshape(-1, tokens.shape[2])
-    all_weights = all_weights.reshape(-1, all_weights.shape[2])
+    proj, w_out = lax.optimization_barrier((proj, w_out))
     full_out = lax.all_gather(w_out, "sp", axis=1, tiled=True)
-    proj = jnp.dot(tokens, all_weights, preferred_element_type=jnp.float32).astype(jnp.bfloat16)
-    extent = tokens.shape[0]
-    count = extent // BLOCK
-
-    onward = [(i, i + 1) for i in range(stretches - 1)]
-    back = [(target, source) for source, target in onward]
-    low = lax.ppermute(proj[extent - 1 :, content : content + channels], "sp", onward)
-    high = lax.ppermute(proj[:1, content : content + channels], "sp", back)
-    edges = jnp.concatenate([low, high], axis=0)
 
     taps = jnp.concatenate([conv_value, conv_state_in, conv_state_out], axis=1)
     padding = ((0, 0), (0, spare))

time: 226 us -> 208 us (0.920)
  matrix products: 11.5 us -> 0 us
  starting transfers between devices: 5.88 us -> 0.03 us
    dot_general x1 -> x0, matrix products: 11.5 us -> none  [on_device(): jnp.dot(tokens, all_weights, preferred_element_type=jnp.float32)]
    ppermute x2 -> x0, starting transfers between devices: 5.84 us -> none  [the longest x1 3.37 us: on_device(): lax.ppermute(proj[extent - 1:, content:content + channels], 'sp', onward)]
    pallas_call x1, Pallas kernels: 76.8 us -> 79.8 us  [on_device(): remote_call(functools.partial(gather_kernel, stretches, parts), (jax.Shap...]
  transfers between devices with their start and end apart: 3 -> 1, of which waited for: 1 -> 0; matrix products, arithmetic and copies ran while one was open for 1% -> 1% of each run, Pallas kernels for 31% -> 33%
where the time goes in v4:
time: 208 us; the launch traced here: 207 us
  Pallas kernels  183 us (88%)
  between operations  13.5 us (6%)
  local copies, waits for them, and re-layouts  6.34 us (3%)
  other arithmetic  4.69 us (2%)
    pallas_call x1, Pallas kernels, on_device(): remote_call(functools.partial(gather_kernel, stretches, parts), (jax.Shap...  79.8 us
    pallas_call x1, Pallas kernels, on_device(): remote_call(functools.partial(exchange_kernel, stretches, (groups, ratio,...  41.4 us
    pallas_call x1, Pallas kernels, on_device(): remote_call(output_kernel, made((rows_out, features), bf16), 2, [pltpu.VM...  34.2 us
    pallas_call x1, Pallas kernels, on_device(): kernel_call(functools.partial(states_kernel, (groups, ratio, content, sta...  14.3 us
    pallas_call x1, Pallas kernels, on_device(): kernel_call(functools.partial(finish_kernel, (groups, ratio, heads)), mad...  13 us
  transfers between devices with their start and end apart: 1, of which 0 were waited for; matrix products, arithmetic and copies ran while one was open for 1% of the time, Pallas kernels for 33%

profile of v4, /device:TPU:12, one launch (start us, length us, event | category | flops | bytes accessed | tf_op | source)
XLA Modules:
  0.0 207.2 jit_solution(7209307321553942552)
XLA Ops:
  6.5 0.0 copy-start
  6.5 0.0 copy-start.1
  6.5 0.0 copy-start.2
  6.5 0.0 copy-start.3
  6.5 0.0 all-gather.2.cloned.1.call-start
  6.6 1.6 fusion
  8.2 0.8 copy.16
  9.0 0.8 copy.17
  9.8 2.5 %fusion.2.tokens_ref = bf16[256,2048]{1,0:T(8,128)(2,1)} fusion(bf16[256,2048]{1,0:T(8,128)(2,1)} %param.15, f32[2048]{0:T(1024)} %param.16, f32[256]{0:T(256)S(1)} %add_rsqrt_fusion), kind=kLoop, calls=%fused_computation.4 | loop fusion | flops 2097152 | bytes 2106368 | tf_op jit(solution)/shard_map/convert_element_type | solution.py:647
  12.3 0.0 copy-done
  12.3 0.0 copy-done.1
  12.3 0.0 copy-done.2
  12.3 0.0 copy-done.3
  12.3 1.1 concatenate.6.weights_ref
  13.5 0.0 copy-start.6
  13.5 79.8 %shard_map.145 = (bf16[1024,1664]{1,0:T(8,128)(2,1)}, bf16[2,16,1664]{2,1,0:T(8,128)(2,1)}) custom-call(bf16[256,2048]{1,0:T(8,128)(2,1)} %fusion.2.tokens_ref, bf16[256,1664]{1,0:T(8,128)(2,1)} %concatenate.6.weights_ref), custom_call_target="tpu_custom_call" | custom-call | flops 30000001024 | bytes 1048576 | tf_op jit(solution)/shard_map/pallas_call | solution.py:654
  93.3 0.0 all-gather.2.cloned.1.call-update
  93.3 0.0 copy-done.7
  93.3 0.1 reshape.18
  93.4 0.0 copy-done.8
  93.4 0.1 reshape.19
  93.5 0.6 pad.7.offset_ref
  94.1 0.5 pad.8.rate_ref
  94.6 0.0 copy-done.4
  94.6 0.0 copy-done.5
  94.6 0.0 copy-done.6
  94.6 0.6 pad_maximum_fusion.taps_ref
  95.2 14.3 %shard_map.146 = (bf16[1024,512]{1,0:T(8,128)(2,1)}, bf16[1024,256]{1,0:T(8,128)(2,1)}, bf16[1024,256]{1,0:T(8,128)(2,1)}, f32[1024,128]{1,0:T(8,128)}, f32[32,1...) custom-call(bf16[1024,1664]{1,0:T(8,128)(2,1)} %get-tuple-element.20.proj_ref,, ...), custom_call_target="tpu_custom_call" | custom-call | flops 7500000256 | bytes 1048576 | tf_op jit(solution)/shard_map/pallas_call | solution.py:688
  109.5 41.4 %shard_map.147 = (bf16[8,272,256]{2,1,0:T(8,128)(2,1)}, f32[1024,512]{1,0:T(8,128)}) custom-call(bf16[2,272,256]{2,1,0:T(8,128)(2,1)} %get-tuple-element.22.sent_ref, bf16[1024,512]{1,0:T(8,128)(2,1)} %get-tuple-element.23.signal_ref, bf16[1024,256]{1,0:T(8,128)(2,1)} %get-tuple-element.24.inward_ref, bf16[1024,256]{1,0:T(8,128)(2,1)} %get-tuple-element.25.outward_ref, ...), custom_call_target="tpu_custom_call" | custom-call | flops 30000001024 | bytes 1048576 | tf_op jit(solution)/shard_map/pallas_call | solution.py:703
  150.9 13.0 %shard_map.148.mixed_ref = bf16[1024,512]{1,0:T(8,128)(2,1)} custom-call(bf16[8,272,256]{2,1,0:T(8,128)(2,1)} %get-tuple-element.28.gathered_ref, f32[2,8,128,512]{3,2,1,0:T(8,128)} %get-tuple-element.29.block_states_ref, f32[2,8,1,512]{3,2,1,0:T(1,128)} %get-tuple-element.30.block_logs_ref, bf16[1024,256]{1,0:T(8,128)(2,1)} %get-tuple-element.25.outward_ref, ...), custom_call_target="tpu_custom_call" | custom-call | flops 7500000256 | bytes 1048576 | tf_op jit(solution)/shard_map/pallas_call | solution.py:710
  163.9 34.2 %shard_map.149 = bf16[256,2048]{1,0:T(8,128)(2,1)} custom-call(bf16[1024,512]{1,0:T(8,128)(2,1)} %shard_map.148.mixed_ref, bf16[512,2048]{1,0:T(8,128)(2,1)} %all-gather.2.cloned.1.call-done.weights_ref), custom_call_target="tpu_custom_call" | custom-call | flops 30000001024 | bytes 1048576 | tf_op jit(solution)/shard_map/pallas_call | solution.py:729
  198.1 2.3 %copy.19 = bf16[256,2048]{1,0:T(8,128)(2,1)} copy(bf16[256,2048]{1,0:T(8,128)(2,1)} %shard_map.149) | data formatting | bytes 2097152
  (7 shorter events, 0.0 us)
Async XLA Ops:
  6.5 5.8 %copy-start = (bf16[256,512]{1,0:T(8,128)(2,1)S(1)}, bf16[256,512]{1,0:T(8,128)(2,1)}, u32[]{:S(2)}) copy-start(bf16[256,512]{1,0:T(8,128)(2,1)} %param.17) | copy-start | bytes 786436
  6.5 5.8 %copy-start.1 = (bf16[256,512]{1,0:T(8,128)(2,1)S(1)}, bf16[256,512]{1,0:T(8,128)(2,1)}, u32[]{:S(2)}) copy-start(bf16[256,512]{1,0:T(8,128)(2,1)} %param.18) | copy-start | bytes 786436
  6.5 5.8 %copy-start.2 = (bf16[256,256]{1,0:T(8,128)(2,1)S(1)}, bf16[256,256]{1,0:T(8,128)(2,1)}, u32[]{:S(2)}) copy-start(bf16[256,256]{1,0:T(8,128)(2,1)} %param.19) | copy-start | bytes 393220
  6.5 5.8 %copy-start.3 = (bf16[256,256]{1,0:T(8,128)(2,1)S(1)}, bf16[256,256]{1,0:T(8,128)(2,1)}, u32[]{:S(2)}) copy-start(bf16[256,256]{1,0:T(8,128)(2,1)} %param.20) | copy-start | bytes 393220
  6.5 157.3 %all-gather.2.cloned.1.call-start = ((), (), s32[]{:S(2)}) async-start(), calls=%async_computation | async-start | bytes 2359296 | tf_op jit(solution)/shard_map/all_gather | solution.py:677
  13.5 79.9 %copy-start.7 = (f32[2,8]{1,0:T(2,128)S(1)}, f32[2,8]{1,0:T(2,128)}, u32[]{:S(2)}) copy-start(f32[2,8]{1,0:T(2,128)} %param.23) | copy-start | bytes 196
  13.5 80.0 %copy-start.8 = (f32[2,8]{1,0:T(2,128)S(1)}, f32[2,8]{1,0:T(2,128)}, u32[]{:S(2)}) copy-start(f32[2,8]{1,0:T(2,128)} %param.24) | copy-start | bytes 196
  13.5 81.2 %copy-start.4 = (f32[3,512]{1,0:T(4,128)S(1)}, f32[3,512]{1,0:T(4,128)}, u32[]{:S(2)}) copy-start(f32[3,512]{1,0:T(4,128)} %param.25) | copy-start | bytes 18436
  13.5 81.2 %copy-start.5 = (f32[3,256]{1,0:T(4,128)S(1)}, f32[3,256]{1,0:T(4,128)}, u32[]{:S(2)}) copy-start(f32[3,256]{1,0:T(4,128)} %param.27) | copy-start | bytes 9220
  13.5 81.2 %copy-start.6 = (f32[3,256]{1,0:T(4,128)S(1)}, f32[3,256]{1,0:T(4,128)}, u32[]{:S(2)}) copy-start(f32[3,256]{1,0:T(4,128)} %param.26) | copy-start | bytes 9220
Sparse Core Ops, SparseCore 0:
  93.5 63.9 all-gather.1

commit v5 on v4

--- a/solution.py
+++ b/solution.py
@@ -132,7 +132,7 @@
             )
         return 0
 
-    lax.fori_loop(0, count, block, 0)
+    lax.fori_loop(0, count, block, 0, unroll=2)
     logs_total[...] = jnp.zeros_like(logs_total)
     for group in range(groups):
 
@@ -210,7 +210,7 @@
                 )
         return 0
 
-    lax.fori_loop(0, count, block, 0)
+    lax.fori_loop(0, count, block, 0, unroll=2)
 
 
 def finish_kernel(
@@ -265,7 +265,7 @@
                 + block_states_ref[group, at][:, span:]
             )
 
-        lax.fori_loop(0, count, back, behind)
+        lax.fori_loop(0, count, back, behind, unroll=2)
 
         def onward(at, state):
             here = pl.ds(pl.multiple_of(at * BLOCK, BLOCK), BLOCK)
@@ -284,7 +284,7 @@
                 + block_states_ref[group, at][:, :span]
             )
 
-        lax.fori_loop(0, count, onward, ahead)
+        lax.fori_loop(0, count, onward, ahead, unroll=2)
 
 
 def ring_place(index, count):
@@ -644,6 +644,7 @@
         ],
         axis=1,
     )
+    full_out = lax.all_gather(w_out, "sp", axis=1, tiled=True)
     normed = (rms_rows(input_activations) * norm_gain).astype(jnp.bfloat16)
     parts = lax.axis_size("tp")
     dma = pltpu.SemaphoreType.DMA
@@ -673,8 +674,6 @@
         ],
         1,
     )(normed, weights)
-    proj, w_out = lax.optimization_barrier((proj, w_out))
-    full_out = lax.all_gather(w_out, "sp", axis=1, tiled=True)
 
     taps = jnp.concatenate([conv_value, conv_state_in, conv_state_out], axis=1)
     padding = ((0, 0), (0, spare))

time: 208 us -> 222 us (1.067)
  Pallas kernels: 183 us -> 196 us
    pallas_call x1, Pallas kernels: 79.8 us -> 105 us  [on_device(): remote_call(functools.partial(gather_kernel, stretches, parts), (jax.Shap...]
    pallas_call x1, Pallas kernels: 41.4 us -> 30 us  [on_device(): remote_call(functools.partial(exchange_kernel, stretches, (groups, ratio,...]
  transfers between devices with their start and end apart: 1 -> 1, of which waited for: 0 -> 0; matrix products, arithmetic and copies ran while one was open for 1% -> 4% of each run, Pallas kernels for 33% -> 73%
where the time goes in v5:
time: 222 us
  Pallas kernels  196 us (88%)
  between operations  13.5 us (6%)
  local copies, waits for them, and re-layouts  7.76 us (3%)
  other arithmetic  4.09 us (2%)
    pallas_call x1, Pallas kernels, on_device(): remote_call(functools.partial(gather_kernel, stretches, parts), (jax.Shap...  105 us
    pallas_call x1, Pallas kernels, on_device(): remote_call(output_kernel, made((rows_out, features), bf16), 2, [pltpu.VM...  34.2 us
    pallas_call x1, Pallas kernels, on_device(): remote_call(functools.partial(exchange_kernel, stretches, (groups, ratio,...  30 us
    pallas_call x1, Pallas kernels, on_device(): kernel_call(functools.partial(states_kernel, (groups, ratio, content, sta...  14.2 us
    pallas_call x1, Pallas kernels, on_device(): kernel_call(functools.partial(finish_kernel, (groups, ratio, heads)), mad...  13 us
  transfers between devices with their start and end apart: 1, of which 0 were waited for; matrix products, arithmetic and copies ran while one was open for 4% of the time, Pallas kernels for 73%

profile of v5, /device:TPU:12, one launch (start us, length us, event | category | flops | bytes accessed | tf_op | source)
XLA Modules:
  0.0 222.1 jit_solution(7157692209271489003)
XLA Ops:
  6.5 0.0 copy-start
  6.5 0.0 copy-start.1
  6.5 0.0 copy-start.2
  6.5 0.0 copy-start.3
  6.5 0.0 copy-start.4
  6.5 0.0 all-gather.2.cloned.1.call-start
  6.6 0.7 all-gather.2.cloned.1.call-update
  7.3 1.5 fusion
  8.8 0.8 copy.16
  9.6 0.8 copy.17
  10.4 0.8 reshape.18
  11.2 0.8 reshape.19
  11.9 0.6 pad.7.offset_ref
  12.5 0.6 pad.8.rate_ref
  13.1 0.0 copy-done
  13.1 2.0 fusion.2.tokens_ref
  15.1 0.0 copy-done.1
  15.1 0.0 copy-done.2
  15.1 0.0 copy-done.3
  15.1 0.0 copy-done.4
  15.1 1.1 concatenate.6.weights_ref
  16.2 0.0 copy-start.5
  16.3 104.6 %shard_map.145 = (bf16[1024,1664]{1,0:T(8,128)(2,1)}, bf16[2,16,1664]{2,1,0:T(8,128)(2,1)}) custom-call(bf16[256,2048]{1,0:T(8,128)(2,1)} %fusion.2.tokens_ref, bf16[256,1664]{1,0:T(8,128)(2,1)} %concatenate.6.weights_ref), custom_call_target="tpu_custom_call" | custom-call | flops 30000001024 | bytes 1048576 | tf_op jit(solution)/shard_map/pallas_call | solution.py:655
  120.9 0.0 copy-done.5
  120.9 0.0 copy-done.6
  120.9 0.0 copy-done.7
  120.9 0.6 pad_maximum_fusion.taps_ref
  121.5 14.2 %shard_map.146 = (bf16[1024,512]{1,0:T(8,128)(2,1)}, bf16[1024,256]{1,0:T(8,128)(2,1)}, bf16[1024,256]{1,0:T(8,128)(2,1)}, f32[1024,128]{1,0:T(8,128)}, f32[32,1...) custom-call(bf16[1024,1664]{1,0:T(8,128)(2,1)} %get-tuple-element.17.proj_ref,, ...), custom_call_target="tpu_custom_call" | custom-call | flops 7500000256 | bytes 1048576 | tf_op jit(solution)/shard_map/pallas_call | solution.py:687
  135.7 30.0 %shard_map.147 = (bf16[8,272,256]{2,1,0:T(8,128)(2,1)}, f32[1024,512]{1,0:T(8,128)}) custom-call(bf16[2,272,256]{2,1,0:T(8,128)(2,1)} %get-tuple-element.19.sent_ref, bf16[1024,512]{1,0:T(8,128)(2,1)} %get-tuple-element.20.signal_ref, bf16[1024,256]{1,0:T(8,128)(2,1)} %get-tuple-element.21.inward_ref, bf16[1024,256]{1,0:T(8,128)(2,1)} %get-tuple-element.22.outward_ref, ...), custom_call_target="tpu_custom_call" | custom-call | flops 30000001024 | bytes 1048576 | tf_op jit(solution)/shard_map/pallas_call | solution.py:702
  165.7 13.0 %shard_map.148.mixed_ref = bf16[1024,512]{1,0:T(8,128)(2,1)} custom-call(bf16[8,272,256]{2,1,0:T(8,128)(2,1)} %get-tuple-element.25.gathered_ref, f32[2,8,128,512]{3,2,1,0:T(8,128)} %get-tuple-element.26.block_states_ref, f32[2,8,1,512]{3,2,1,0:T(1,128)} %get-tuple-element.27.block_logs_ref, bf16[1024,256]{1,0:T(8,128)(2,1)} %get-tuple-element.22.outward_ref, ...), custom_call_target="tpu_custom_call" | custom-call | flops 7500000256 | bytes 1048576 | tf_op jit(solution)/shard_map/pallas_call | solution.py:709
  178.7 34.2 %shard_map.149 = bf16[256,2048]{1,0:T(8,128)(2,1)} custom-call(bf16[1024,512]{1,0:T(8,128)(2,1)} %shard_map.148.mixed_ref, bf16[512,2048]{1,0:T(8,128)(2,1)} %all-gather.2.cloned.1.call-done.weights_ref), custom_call_target="tpu_custom_call" | custom-call | flops 30000001024 | bytes 1048576 | tf_op jit(solution)/shard_map/pallas_call | solution.py:728
  212.9 2.3 %copy.19 = bf16[256,2048]{1,0:T(8,128)(2,1)} copy(bf16[256,2048]{1,0:T(8,128)(2,1)} %shard_map.149) | data formatting | bytes 2097152
  (5 shorter events, 0.0 us)
Async XLA Ops:
  6.5 6.6 %copy-start = (bf16[256,2048]{1,0:T(8,128)(2,1)S(1)}, bf16[256,2048]{1,0:T(8,128)(2,1)}, u32[]{:S(2)}) copy-start(bf16[256,2048]{1,0:T(8,128)(2,1)} %param.15) | copy-start | bytes 3145732
  6.5 8.6 %copy-start.1 = (bf16[256,512]{1,0:T(8,128)(2,1)S(1)}, bf16[256,512]{1,0:T(8,128)(2,1)}, u32[]{:S(2)}) copy-start(bf16[256,512]{1,0:T(8,128)(2,1)} %param.17) | copy-start | bytes 786436
  6.5 8.6 %copy-start.2 = (bf16[256,512]{1,0:T(8,128)(2,1)S(1)}, bf16[256,512]{1,0:T(8,128)(2,1)}, u32[]{:S(2)}) copy-start(bf16[256,512]{1,0:T(8,128)(2,1)} %param.18) | copy-start | bytes 786436
  6.5 8.6 %copy-start.3 = (bf16[256,256]{1,0:T(8,128)(2,1)S(1)}, bf16[256,256]{1,0:T(8,128)(2,1)}, u32[]{:S(2)}) copy-start(bf16[256,256]{1,0:T(8,128)(2,1)} %param.19) | copy-start | bytes 393220
  6.5 8.6 %copy-start.4 = (bf16[256,256]{1,0:T(8,128)(2,1)S(1)}, bf16[256,256]{1,0:T(8,128)(2,1)}, u32[]{:S(2)}) copy-start(bf16[256,256]{1,0:T(8,128)(2,1)} %param.20) | copy-start | bytes 393220
  6.5 172.2 %all-gather.2.cloned.1.call-start = ((), (), s32[]{:S(2)}) async-start(), calls=%async_computation | async-start | bytes 2359296 | tf_op jit(solution)/shard_map/all_gather | solution.py:647
  16.2 104.6 %copy-start.5 = (f32[3,512]{1,0:T(4,128)S(1)}, f32[3,512]{1,0:T(4,128)}, u32[]{:S(2)}) copy-start(f32[3,512]{1,0:T(4,128)} %param.25) | copy-start | bytes 18436
  16.2 104.6 %copy-start.6 = (f32[3,256]{1,0:T(4,128)S(1)}, f32[3,256]{1,0:T(4,128)}, u32[]{:S(2)}) copy-start(f32[3,256]{1,0:T(4,128)} %param.27) | copy-start | bytes 9220
  16.3 104.6 %copy-start.7 = (f32[3,256]{1,0:T(4,128)S(1)}, f32[3,256]{1,0:T(4,128)}, u32[]{:S(2)}) copy-start(f32[3,256]{1,0:T(4,128)} %param.26) | copy-start | bytes 9220
Sparse Core Ops, SparseCore 0:
  9.4 70.6 all-gather.1
